TPU v7x, 512 devices: a whole 4x4x16 slice. The times are simulated.
512 devices in a mesh: fs: 16 (over z), rep: 4 (over y), tp: 8 (over x, core).
Axes of the slice: x: 4, y: 4, z: 16, core: 2. Of those that a mesh axis runs over, the one named last changes fastest.
Arguments:
- normed: bfloat16 [40960, 2048], P(('fs', 'rep')), may hold values from -150 to 150
- rec_cot: bfloat16 [40960, 2048], P(('fs', 'rep'), 'tp'), may hold values from -0.74115883 to 0.74115883
- conv_out: bfloat16 [40960, 2048], P(('fs', 'rep'), 'tp'), may hold values from -6 to 6
- gate_cot: bfloat16 [40960, 2048], P(('fs', 'rep'), 'tp'), may hold values from -0.029541016 to 0.029541016
- rec_weight: float32 [2048, 2048], P('fs', 'tp'), may hold values from -0.125 to 0.125
- rec_moment: float32 [2048, 2048], P('fs', 'tp'), may hold values from -6 to 6
- rec_right: bfloat16 [2048, 256], P('tp'), may hold values from -1 to 2
- gate_weight: float32 [8, 256, 256], P('tp', 'fs'), may hold values from -0.375 to 0.375
- gate_moment: float32 [8, 256, 256], P('tp', 'fs'), may hold values from -6 to 6
- gate_left: bfloat16 [8, 256, 256], P('tp', 'fs'), may hold values from -1 to 2
- gate_right: bfloat16 [8, 256, 256], P('tp'), may hold values from -1 to 2
Outputs:
- rec_weight_new: float32 [2048, 2048], P('fs', 'tp')
- rec_moment_new: float32 [2048, 2048], P('fs', 'tp')
- rec_step: float32 [2048, 2048], P('fs', 'tp')
- rec_copy: bfloat16 [2048, 2048], P('fs', 'tp')
- gate_weight_new: float32 [8, 256, 256], P('tp', 'fs')
- gate_moment_new: float32 [8, 256, 256], P('tp', 'fs')
- gate_step: float32 [8, 256, 256], P('tp', 'fs')
- gate_copy: bfloat16 [8, 256, 256], P('tp', 'fs')
All inputs are finite; a program needn't handle non-finite values.
Results may differ from a plain program's by a relative error of at most 0.001.
Values sent between devices are 32-bit elements; how exact they have to be, the bound alone decides.
No kernel may reach another device: no remote copies, remote signals or barrier semaphores. Data moves between devices by JAX's collectives and lax.ppermute only.
A program may use at most 64 MiB of HBM per device.

v0:
```python
import functools

import jax
import jax.numpy as jnp
from jax import lax
from jax.sharding import Mesh
from jax.sharding import PartitionSpec as P

FS_TP = ("fs", "tp_0", "tp_1")
TP = ("tp_0", "tp_1")


BETA = 0.9
LEARN_RATE = 0.02
EPSILON = 1e-06


def sent_to_all(value, axis):
    copies = jnp.broadcast_to(value, (lax.axis_size(axis), *value.shape))
    return lax.all_to_all(copies, axis, split_axis=0, concat_axis=0, tiled=True)


def over_copies(value, axis):
    everything = sent_to_all(value, axis)
    return jnp.sum(everything, axis=0)


def split_up(value, dim, devices):
    before, after = (value.shape[:dim], value.shape[dim + 1 :])
    return jnp.moveaxis(value.reshape(*before, devices, -1, *after), dim, 0)


def summed_on_arrival(value, axis, dim):
    tiles = split_up(value, dim, lax.axis_size(axis))
    arrived = lax.all_to_all(tiles, axis, split_axis=0, concat_axis=0, tiled=True)
    return arrived.sum(axis=0)


def joined_along(tiles, dim):
    tiles = jnp.moveaxis(tiles, 0, dim)
    shape = tiles.shape
    return tiles.reshape(*shape[:dim], shape[dim] * shape[dim + 1], *shape[dim + 2 :])


def gather_directly(value, axis, dim):
    tiles = sent_to_all(value, axis)
    return joined_along(tiles, dim)


def one_axis_at_a_time(value, axes):
    return functools.reduce(lax.psum, axes, value)


def precondition_right(gradient, factor):
    row_count = gradient.shape[0]
    block_size = factor.shape[1]
    blocks = factor.shape[0] // block_size
    shaped = gradient.reshape(row_count, blocks, block_size)
    factors = factor.astype(jnp.float32).reshape(blocks, block_size, block_size)
    result = jnp.einsum("rbi,bij->rbj", shaped, factors, precision=lax.Precision.HIGHEST)
    return result.reshape(row_count, blocks * block_size)


def shards(
    normed,
    rec_cot,
    conv_out,
    gate_cot,
    rec_weight,
    rec_moment,
    rec_right,
    gate_weight,
    gate_moment,
    gate_left,
    gate_right,
):
    token_count = normed.shape[0]
    columns = normed
    partial_rows = lax.psum_scatter(
        lax.dot_general(
            columns, rec_cot, (((0,), (0,)), ((), ())), preferred_element_type=jnp.float32
        ),
        "fs",
        scatter_dimension=0,
        tiled=True,
    )
    rec_grad = over_copies(partial_rows, "rep")
    rec_pre = precondition_right(rec_grad, rec_right)
    block_count, own_rows, block_size = gate_weight.shape
    conv_blocks = conv_out.reshape(token_count, block_count, block_size)
    cot_blocks = gate_cot.reshape(token_count, block_count, block_size)
    gate_term = jnp.einsum(
        "tbi,tbj->bij", conv_blocks, cot_blocks, preferred_element_type=jnp.float32
    )
    right_factor = gate_right.astype(jnp.float32)
    left_factor = gate_left.astype(jnp.float32)
    part_grad = summed_on_arrival(gate_term, "fs", 1)
    gate_grad = over_copies(part_grad, "rep")
    right_done = jnp.einsum(
        "bij,bjk->bik", gate_grad, right_factor, precision=lax.Precision.HIGHEST
    )
    columns = left_factor
    gate_pre = jnp.einsum(
        "bri,bik->brk",
        columns,
        gather_directly(right_done, "fs", 1),
        precision=lax.Precision.HIGHEST,
    )
    rec_moment_new = BETA * rec_moment + rec_pre
    gate_moment_new = BETA * gate_moment + gate_pre
    totals = (
        one_axis_at_a_time(jnp.sum(rec_grad * rec_grad), FS_TP),
        one_axis_at_a_time(jnp.sum(rec_moment_new * rec_moment_new), FS_TP),
        one_axis_at_a_time(jnp.sum(gate_grad * gate_grad), FS_TP),
        one_axis_at_a_time(jnp.sum(gate_moment_new * gate_moment_new), FS_TP),
    )
    rec_scale = jnp.sqrt(totals[0]) / jnp.sqrt(totals[1] + EPSILON)
    gate_scale = jnp.sqrt(totals[2]) / jnp.sqrt(totals[3] + EPSILON)
    rec_taken = LEARN_RATE * rec_scale * rec_moment_new
    gate_taken = LEARN_RATE * gate_scale * gate_moment_new
    rec_new = rec_weight - rec_taken
    gate_new = gate_weight - gate_taken
    return (
        rec_new,
        rec_moment_new,
        rec_taken,
        rec_new.astype(jnp.bfloat16),
        gate_new,
        gate_moment_new,
        gate_taken,
        gate_new.astype(jnp.bfloat16),
    )


def solution(mesh):
    split = Mesh(
        mesh.devices.reshape(mesh.shape["fs"], mesh.shape["rep"], 4, 2),
        ("fs", "rep", "tp_0", "tp_1"),
    )
    placed = (
        P(("fs", "rep"), None),
        P(("fs", "rep"), TP),
        P(("fs", "rep"), TP),
        P(("fs", "rep"), TP),
        P("fs", TP),
        P("fs", TP),
        P(TP, None),
        P(TP, "fs", None),
        P(TP, "fs", None),
        P(TP, "fs", None),
        P(TP, None, None),
    )
    return jax.shard_map(
        shards,
        mesh=split,
        in_specs=placed,
        out_specs=(
            P("fs", TP),
            P("fs", TP),
            P("fs", TP),
            P("fs", TP),
            P(TP, "fs", None),
            P(TP, "fs", None),
            P(TP, "fs", None),
            P(TP, "fs", None),
        ),
        check_vma=False,
    )
```

profile of v0, /device:TPU:1, one launch (start us, length us, event | category | flops | bytes accessed | tf_op | source)
XLA Modules:
  0.0 176.0 jit_solution(7246339247438781768)
XLA Ops:
  7.2 0.0 copy-start
  7.2 0.0 reduce-scatter.2.cloned.1.call-start
  7.2 1.7 copy-done
  8.9 3.3 %fusion.7 = f32[2048,256]{1,0:T(8,128)} fusion(bf16[640,2048]{1,0:T(8,128)(2,1)S(1)} %copy-done, bf16[640,256]{1,0:T(8,128)(2,1)} %param.12), kind=kOutput, calls=%fused_computation.16 | convolution fusion | flops 671088640 | bytes 5046272 | tf_op jit(solution)/shard_map/dot_general | solution.py:80
  12.3 0.0 copy-start.2
  12.3 0.0 copy-start.3
  12.3 0.0 reduce-scatter.2.cloned.1.call-update
  12.3 1.2 copy.23
  13.5 0.0 copy-done.2
  13.5 0.3 convolution_bitcast_fusion
  13.8 29.3 %all_to_all.20 = f32[16,1,16,256]{3,2,1,0:T(8,128)S(1)} all-to-all(f32[16,1,16,256]{3,2,1,0:T(8,128)S(1)} %convolution_bitcast_fusion), channel_id=1, replica_groups=mesh['fs'=16,'rep'=4,'tp_0'=4,'tp_1'=2] {'fs'}, dimensions={0} | all-to-all | bytes 524288 | tf_op jit(solution)/shard_map/all_to_all | solution.py:35
  43.1 8.5 %all_to_all.21 = f32[4,1,16,256]{3,2,1,0:T(8,128)S(1)} all-to-all(f32[4,1,16,256]{3,2,1,0:T(8,128)S(1)} %broadcast_in_dim.10), channel_id=1, replica_groups=mesh['fs'=16,'rep'=4,'tp_0'=4,'tp_1'=2] {'rep'}, dimensions={0} | all-to-all | bytes 131072 | tf_op jit(solution)/shard_map/all_to_all | solution.py:20
  51.6 0.0 copy-done.3
  51.6 0.1 fusion.2
  51.8 0.1 broadcast_in_dim.11
  51.8 26.4 %all_to_all.22 = f32[16,1,16,256]{3,2,1,0:T(8,128)S(1)} all-to-all(f32[16,1,16,256]{3,2,1,0:T(8,128)S(1)} %broadcast_in_dim.11), channel_id=1, replica_groups=mesh['fs'=16,'rep'=4,'tp_0'=4,'tp_1'=2] {'fs'}, dimensions={0} | all-to-all | bytes 524288 | tf_op jit(solution)/shard_map/all_to_all | solution.py:20
  78.2 16.4 %reduce-scatter.2.cloned.1.call-done = f32[128,256]{1,0:T(8,128)} async-done(((f32[2048,256]{1,0:T(8,128)}), f32[128,256]{1,0:T(8,128)}) %reduce-scatter.2.cloned.1.call-update) | async-done | bytes 131088 | tf_op jit(solution)/shard_map/reduce_scatter | solution.py:79
  94.6 1.7 broadcast_in_dim.9
  96.3 4.8 %all-to-all-start = ((f32[4,128,256]{2,1,0:T(8,128)}), f32[4,128,256]{2,1,0:T(8,128)S(1)}, u32[]{:S(2)}, u32[]{:S(2)}) async-start(f32[4,128,256]{2,1,0:T(8,128)} %broadcast_in_dim.9), calls=%async_computation.1 | async-start | bytes 1048576 | tf_op jit(solution)/shard_map/all_to_all | solution.py:20
  101.1 0.6 multiply_reduce_fusion.3
  101.7 1.6 multiply_reduce_fusion.2
  103.3 0.0 copy-start.4
  103.3 4.8 %all-to-all-done = f32[4,128,256]{2,1,0:T(8,128)S(1)} async-done(((f32[4,128,256]{2,1,0:T(8,128)}), f32[4,128,256]{2,1,0:T(8,128)S(1)}, u32[]{:S(2)}, u32[]{:S(2)}) %all-to-all-start) | async-done | bytes 524320 | tf_op jit(solution)/shard_map/all_to_all | solution.py:20
  108.1 0.6 multiply_reduce_fusion.1
  108.8 1.8 %multiply_reduce_fusion = (f32[]{:T(128)}, f32[128,256]{1,0:T(8,128)S(1)}) fusion(f32[128,256]{1,0:T(8,128)S(1)} %reduce_sum.63, bf16[256,256]{1,0:T(8,128)(2,1)} %param.17, f32[128,256]{1,0:T(8,128)} %param.16), kind=kOutput, calls=%fused_computation.7 | convolution fusion | flops 100794368 | bytes 524292 | tf_op jit(solution)/shard_map/rbi,bij->rbj/dot_general | solution.py:60
  110.6 22.1 %all-reduce = (f32[]{:T(128)}, f32[]{:T(128)}, f32[]{:T(128)}, f32[]{:T(128)}) all-reduce(f32[]{:T(128)} %multiply_reduce_fusion.1, f32[]{:T(128)} %get-tuple-element.26, f32[]{:T(128)} %multiply_reduce_fusion.3, f32[]{:T(128)} %get-tuple-element.28), channel_id=1, replica_groups=mesh['fs'=16,'rep'=4,'tp_0'=4,'tp_1'=2] {'fs'}, use_global_device_ids=true, to_apply=%region_3.0 | all-reduce | flops 4 | bytes 32 | tf_op jit(solution)/shard_map/psum | solution.py:51
  132.7 8.8 %all-reduce.1 = (f32[]{:T(128)}, f32[]{:T(128)}, f32[]{:T(128)}, f32[]{:T(128)}) all-reduce(f32[]{:T(128)} %get-tuple-element.8, f32[]{:T(128)} %get-tuple-element.9, f32[]{:T(128)} %get-tuple-element.10, f32[]{:T(128)} %get-tuple-element.11), channel_id=1, replica_groups=mesh['fs'=16,'rep'=4,'tp_0'=4,'tp_1'=2] {'tp_0'}, use_global_device_ids=true, to_apply=%region_4.0 | all-reduce | flops 4 | bytes 32 | tf_op jit(solution)/shard_map/psum | solution.py:51
  141.4 22.0 %all-reduce.2 = (f32[]{:T(128)}, f32[]{:T(128)}, f32[]{:T(128)}, f32[]{:T(128)}) all-reduce(f32[]{:T(128)} %get-tuple-element.12, f32[]{:T(128)} %get-tuple-element.13, f32[]{:T(128)} %get-tuple-element.14, f32[]{:T(128)} %get-tuple-element.15), channel_id=1, replica_groups=mesh['fs'=16,'rep'=4,'tp_0'=4,'tp_1'=2] {'tp_1'}, use_global_device_ids=true, to_apply=%region_5.0 | all-reduce | flops 4 | bytes 32 | tf_op jit(solution)/shard_map/psum | solution.py:51
  166.2 1.3 fusion.5
  167.5 1.6 fusion.6
  169.1 0.0 copy-done.4
  169.2 0.0 copy-done.1
  (5 shorter events, 0.1 us)
Async XLA Ops:
  7.2 1.7 copy-start
  7.2 87.4 %reduce-scatter.2.cloned.1.call-start = ((), (), s32[]{:S(2)}) async-start(), calls=%async_computation.5 | async-start | bytes 2228224 | tf_op jit(solution)/shard_map/reduce_scatter | solution.py:79
  12.3 1.3 copy-start.2
  12.3 39.4 %copy-start.3 = (bf16[1,256,256]{2,1,0:T(8,128)(2,1)S(1)}, bf16[1,256,256]{2,1,0:T(8,128)(2,1)}, u32[]{:S(2)}) copy-start(bf16[1,256,256]{2,1,0:T(8,128)(2,1)} %param.21) | copy-start | bytes 393220
  96.3 11.7 %all-to-all-start = ((f32[4,128,256]{2,1,0:T(8,128)}), f32[4,128,256]{2,1,0:T(8,128)S(1)}, u32[]{:S(2)}, u32[]{:S(2)}) async-start(f32[4,128,256]{2,1,0:T(8,128)} %broadcast_in_dim.9), calls=%async_computation.1 | async-start | bytes 1048576 | tf_op jit(solution)/shard_map/all_to_all | solution.py:20
  103.3 65.8 %copy-start.4 = (f32[1,16,256]{2,1,0:T(8,128)}, f32[1,16,256]{2,1,0:T(8,128)S(1)}, u32[]{:S(2)}) copy-start(f32[1,16,256]{2,1,0:T(8,128)S(1)} %get-tuple-element.29) | copy-start | bytes 49156
  110.6 58.6 %copy-start.1 = (f32[128,256]{1,0:T(8,128)}, f32[128,256]{1,0:T(8,128)S(1)}, u32[]{:S(2)}) copy-start(f32[128,256]{1,0:T(8,128)S(1)} %get-tuple-element.27) | copy-start | bytes 393220
Sparse Core Ops, SparseCore 0:
  12.4 82.1 reduce-scatter.1
where the time goes:
time: 177 us; the launch traced here: 176 us
  blocking collectives  117 us (66%)
  waiting for transfers between devices  21.2 us (12%)
  between operations  16.9 us (10%)
  matrix products  7.11 us (4%)
  starting transfers between devices  4.84 us (3%)
  local copies, waits for them, and re-layouts  4.74 us (3%)
  other arithmetic  4.27 us (2%)
    psum x3, blocking collectives, one_axis_at_a_time(): return functools.reduce(lax.psum, axes, value)  52.9 us
    all_to_all x2, blocking collectives, sent_to_all(): return lax.all_to_all(copies, axis, split_axis=0, concat_axis=0, tiled=True)  34.8 us
    all_to_all x1, blocking collectives, summed_on_arrival(): lax.all_to_all(tiles, axis, split_axis=0, concat_axis=0, tiled=True)  29.3 us
    reduce_scatter x1, waiting for transfers between devices, shards(): lax.psum_scatter(lax.dot_general(columns, rec_cot, (((0,), (0,)), ((), ()...  16.4 us
    all_to_all x1, starting transfers between devices, sent_to_all(): return lax.all_to_all(copies, axis, split_axis=0, concat_axis=0, tiled=True)  4.8 us
    all_to_all x1, waiting for transfers between devices, sent_to_all(): return lax.all_to_all(copies, axis, split_axis=0, concat_axis=0, tiled=True)  4.77 us
  transfers between devices with their start and end apart: 2, of which 2 were waited for; matrix products, arithmetic and copies ran while one was open for 2% of the time, Pallas kernels for 0%

commit v1 on v0

v1 whole, which is shorter than its diff:
```python
import jax
import jax.numpy as jnp
from jax import lax
from jax.sharding import Mesh
from jax.sharding import PartitionSpec as P

FS = ("fs_hi", "fs_lo")
NEAR = ("fs_lo", "rep")
TP = ("tp_0", "tp_1")

BETA = 0.9
LEARN_RATE = 0.02
EPSILON = 1e-06
F32 = jnp.float32
HIGH = lax.Precision.HIGHEST


def size_of(axes):
    axes = (axes,) if isinstance(axes, str) else axes
    size = 1
    for axis in axes:
        size *= lax.axis_size(axis)
    return size


def exchange(tiles, axes):
    return lax.all_to_all(tiles, axes, split_axis=0, concat_axis=0, tiled=True)


def gathered(value, axes):
    copies = jnp.broadcast_to(value, (size_of(axes), *value.shape))
    return exchange(copies, axes)


def by_owner(rows, hi, lo, rep):
    columns = rows.shape[-1]
    tiles = rows.reshape(hi, lo, rep, -1, columns)
    return tiles.transpose(1, 2, 0, 3, 4).reshape(lo * rep, hi, -1, columns)


def shards(
    normed,
    rec_cot,
    conv_out,
    gate_cot,
    rec_weight,
    rec_moment,
    rec_right,
    gate_weight,
    gate_moment,
    gate_left,
    gate_right,
):
    hi, lo = lax.axis_size("fs_hi"), lax.axis_size("fs_lo")
    rep = lax.axis_size("rep")
    fs = hi * lo
    block = gate_weight.shape[-1]

    left_rows = gate_left[0].astype(F32)
    left = gathered(left_rows, FS).reshape(block, block)

    contract = (((0,), (0,)), ((), ()))
    rec_part = lax.dot_general(normed, rec_cot, contract, preferred_element_type=F32)
    gate_part = lax.dot_general(conv_out, gate_cot, contract, preferred_element_type=F32)
    right = gate_right[0].astype(F32)
    pre_part = jnp.dot(
        jnp.dot(left, gate_part, precision=HIGH), right, precision=HIGH
    )

    tiles = jnp.concatenate(
        [by_owner(v, hi, lo, rep) for v in (rec_part, gate_part, pre_part)], axis=2
    )
    near = exchange(tiles, NEAR).sum(axis=0)
    own = exchange(near, "fs_hi").sum(axis=0)

    full = gathered(own, "rep")
    n_rec, n_gate = rec_part.shape[0] // (fs * rep), block // (fs * rep)
    rec_grad = full[:, :n_rec].reshape(-1, block)
    gate_grad = full[:, n_rec : n_rec + n_gate].reshape(-1, block)
    gate_pre = full[:, n_rec + n_gate :].reshape(-1, block)

    rec_pre = jnp.dot(rec_grad, rec_right.astype(F32), precision=HIGH)
    rec_moment_new = BETA * rec_moment + rec_pre
    gate_moment_new = BETA * gate_moment[0] + gate_pre
    sums = jnp.stack(
        [
            jnp.sum(v * v)
            for v in (rec_grad, rec_moment_new, gate_grad, gate_moment_new)
        ]
    )
    sums = jnp.broadcast_to(sums[:, None], (4, 128))
    sums = gathered(sums, FS).sum(axis=0)
    totals = gathered(sums, TP).sum(axis=0)[:, 0]
    rec_scale = jnp.sqrt(totals[0]) / jnp.sqrt(totals[1] + EPSILON)
    gate_scale = jnp.sqrt(totals[2]) / jnp.sqrt(totals[3] + EPSILON)
    rec_taken = LEARN_RATE * rec_scale * rec_moment_new
    gate_taken = LEARN_RATE * gate_scale * gate_moment_new
    rec_new = rec_weight - rec_taken
    gate_new = gate_weight[0] - gate_taken
    return (
        rec_new,
        rec_moment_new,
        rec_taken,
        rec_new.astype(jnp.bfloat16),
        gate_new[None],
        gate_moment_new[None],
        gate_taken[None],
        gate_new.astype(jnp.bfloat16)[None],
    )


def solution(mesh):
    fs, rep, tp = (mesh.shape[name] for name in ("fs", "rep", "tp"))
    split = Mesh(
        mesh.devices.reshape(fs // 2, 2, rep, tp // 2, 2),
        (*FS, "rep", *TP),
    )
    tokens = (*FS, "rep")
    placed = (
        P(tokens, None),
        P(tokens, TP),
        P(tokens, TP),
        P(tokens, TP),
        P(FS, TP),
        P(FS, TP),
        P(TP, None),
        P(TP, FS, None),
        P(TP, FS, None),
        P(TP, FS, None),
        P(TP, None, None),
    )
    return jax.shard_map(
        shards,
        mesh=split,
        in_specs=placed,
        out_specs=(P(FS, TP),) * 4 + (P(TP, FS, None),) * 4,
        check_vma=False,
    )
```

time: 177 us -> 156 us (0.88)
  blocking collectives: 117 us -> 83.7 us
  starting transfers between devices: 4.84 us -> 26.7 us
  between operations: 16.9 us -> 3.53 us
  other arithmetic: 4.27 us -> 11.7 us
  waiting for transfers between devices: 21.2 us -> 16.7 us
  local copies, waits for them, and re-layouts: 4.74 us -> 7.03 us
    psum x3 -> x0, blocking collectives: 52.9 us -> none  [one_axis_at_a_time(): return functools.reduce(lax.psum, axes, value)]
    all_to_all x1 -> x3, starting transfers between devices: 4.8 us -> 26.7 us  [exchange(): return lax.all_to_all(tiles, axes, split_axis=0, concat_axis=0, tiled=True)]
    all_to_all x3, blocking collectives: 64.1 us -> 83.7 us  [exchange(): return lax.all_to_all(tiles, axes, split_axis=0, concat_axis=0, tiled=True)]
    reduce_scatter x1 -> x0, waiting for transfers between devices: 16.4 us -> none  [shards(): lax.psum_scatter(lax.dot_general(columns, rec_cot, (((0,), (0,)), ((), ()...]
    all_to_all x1 -> x3, waiting for transfers between devices: 4.77 us -> 16.7 us  [exchange(): return lax.all_to_all(tiles, axes, split_axis=0, concat_axis=0, tiled=True)]
    unnamed x11 -> x12, local copies, waits for them, and re-layouts: 2.93 us -> 0.03 us
    another operation x0 -> x1, other arithmetic: none -> 2.66 us  [shards(): jnp.stack([jnp.sum(v * v) for v in (rec_grad, rec_moment_new, gate_grad,...]
    transpose x0 -> x2, local copies, waits for them, and re-layouts: none -> 2.46 us  [by_owner(): return tiles.transpose(1, 2, 0, 3, 4).reshape(lo * rep, hi, -1, columns)]
  transfers between devices with their start and end apart: 2 -> 3, of which waited for: 2 -> 3; matrix products, arithmetic and copies ran while one was open for 2% -> 4% of each run, Pallas kernels for 0% -> 0%
where the time goes in v1:
time: 156 us; the launch traced here: 155 us
  blocking collectives  83.7 us (54%)
  starting transfers between devices  26.7 us (17%)
  waiting for transfers between devices  16.7 us (11%)
  other arithmetic  11.7 us (8%)
  local copies, waits for them, and re-layouts  7.03 us (5%)
  matrix products  5.72 us (4%)
  between operations  3.53 us (2%)
    all_to_all x3, blocking collectives, exchange(): return lax.all_to_all(tiles, axes, split_axis=0, concat_axis=0, tiled=True)  83.7 us
    all_to_all x3, starting transfers between devices, exchange(): return lax.all_to_all(tiles, axes, split_axis=0, concat_axis=0, tiled=True)  26.7 us
    all_to_all x3, waiting for transfers between devices, exchange(): return lax.all_to_all(tiles, axes, split_axis=0, concat_axis=0, tiled=True)  16.7 us
  transfers between devices with their start and end apart: 3, of which 3 were waited for; matrix products, arithmetic and copies ran while one was open for 4% of the time, Pallas kernels for 0%

profile of v1, /device:TPU:1, one launch (start us, length us, event | category | flops | bytes accessed | tf_op | source)
XLA Modules:
  0.0 155.1 jit_solution(11555392444276990373)
XLA Ops:
  0.6 0.9 bitcast_convert_fusion
  1.5 0.8 broadcast_in_dim.6
  2.3 15.7 %all-to-all-start = ((f32[16,16,256]{2,1,0:T(8,128)}), f32[16,16,256]{2,1,0:T(8,128)S(1)}, u32[]{:S(2)}, u32[]{:S(2)}) async-start(f32[16,16,256]{2,1,0:T(8,128)} %broadcast_in_dim.6), calls=%async_computation | async-start | bytes 524288 | tf_op jit(solution)/shard_map/all_to_all | solution.py:27
  18.0 1.4 fusion.10
  19.4 0.8 reshape.76
  20.1 1.0 copy.30
  21.1 2.0 %fusion.9 = f32[2048,256]{1,0:T(8,128)S(1)} fusion(bf16[640,2048]{1,0:T(8,128)(2,1)S(1)} %copy-done, bf16[640,256]{1,0:T(8,128)(2,1)} %param.12), kind=kOutput, calls=%fused_computation.20 | convolution fusion | flops 671088640 | bytes 5046272 | tf_op jit(solution)/shard_map/dot_general | solution.py:63
  23.1 1.5 copy.29
  24.6 7.1 %all-to-all-done = f32[16,16,256]{2,1,0:T(8,128)S(1)} async-done(((f32[16,16,256]{2,1,0:T(8,128)}), f32[16,16,256]{2,1,0:T(8,128)S(1)}, u32[]{:S(2)}, u32[]{:S(2)}) %all-to-all-start) | async-done | bytes 262176 | tf_op jit(solution)/shard_map/all_to_all | solution.py:27
  31.8 1.1 convolution_bitcast_fusion
  32.9 1.0 dot_general.23
  33.9 0.4 fusion
  34.3 0.1 copy.32
  34.4 1.9 %pad_maximum_fusion = f32[8,8,40,256]{3,2,1,0:T(8,128)S(1)} fusion(f32[8,8,4,256]{3,2,1,0:T(4,128)S(1)} %copy.32, f32[8,8,4,256]{3,2,1,0:T(4,128)S(1)} %bitcast.39, f32[8,8,32,256]{3,2,1,0:T(8,128)} %bitcast.37), kind=kLoop, calls=%fused_computation | loop fusion | flops 1310720 | bytes 5242880 | tf_op jit(solution)/shard_map/concatenate | solution.py:70
  36.4 39.0 %all_to_all.30 = f32[8,8,40,256]{3,2,1,0:T(8,128)} all-to-all(f32[8,8,40,256]{3,2,1,0:T(8,128)S(1)} %pad_maximum_fusion), channel_id=1, replica_groups=mesh['fs_hi'=8,'fs_lo'=2,'rep'=4,'tp_0'=4,'tp_1'=2] {'fs_lo','rep'}, dimensions={0} | all-to-all | bytes 5242880 | tf_op jit(solution)/shard_map/all_to_all | solution.py:27
  75.3 2.0 %reduce_sum.72 = f32[8,40,256]{2,1,0:T(8,128)S(1)} reduce(f32[8,8,40,256]{3,2,1,0:T(8,128)} %all_to_all.30, f32[]{:T(128)} %constant.4.clone.1), dimensions={0}, to_apply=%region_0.0 | reduce | flops 573440 | bytes 2949124 | tf_op jit(solution)/shard_map/reduce_sum | solution.py:73
  77.3 27.6 %all_to_all.31 = f32[8,40,256]{2,1,0:T(8,128)S(1)} all-to-all(f32[8,40,256]{2,1,0:T(8,128)S(1)} %reduce_sum.72), channel_id=1, replica_groups=mesh['fs_hi'=8,'fs_lo'=2,'rep'=4,'tp_0'=4,'tp_1'=2] {'fs_hi'}, dimensions={0} | all-to-all | bytes 655360 | tf_op jit(solution)/shard_map/all_to_all | solution.py:27
  105.0 0.7 broadcast_in_dim.7
  105.7 3.3 %all-to-all-start.3 = ((f32[4,40,256]{2,1,0:T(8,128)}), f32[4,40,256]{2,1,0:T(8,128)S(1)}, u32[]{:S(2)}, u32[]{:S(2)}) async-start(f32[4,40,256]{2,1,0:T(8,128)} %broadcast_in_dim.7), calls=%async_computation.3 | async-start | bytes 327680 | tf_op jit(solution)/shard_map/all_to_all | solution.py:27
  109.1 4.9 %all-to-all-done.3 = f32[4,40,256]{2,1,0:T(8,128)S(1)} async-done(((f32[4,40,256]{2,1,0:T(8,128)}), f32[4,40,256]{2,1,0:T(8,128)S(1)}, u32[]{:S(2)}, u32[]{:S(2)}) %all-to-all-start.3) | async-done | bytes 163872 | tf_op jit(solution)/shard_map/all_to_all | solution.py:27
  114.0 0.6 multiply_reduce_fusion.1
  114.6 0.8 multiply_reduce_fusion
  115.5 0.6 fusion.3
  116.1 2.7 %pad_maximum_fusion.1 = f32[4]{0:T(128)S(1)} fusion(f32[1]{0:T(128)} %bitcast.17, f32[1]{0:T(128)} %bitcast.16, f32[1]{0:T(128)} %bitcast.15, f32[1]{0:T(128)} %bitcast.13), kind=kLoop, calls=%fused_computation.15 | loop fusion | flops 12 | bytes 32 | tf_op jit(solution)/shard_map/stack | solution.py:85
  118.7 0.1 broadcast_in_dim_broadcast_in_dim.2
  118.8 17.1 %all_to_all.32 = f32[16,4,128]{2,1,0:T(4,128)S(1)} all-to-all(f32[16,4,128]{2,1,0:T(4,128)S(1)} %broadcast_in_dim_broadcast_in_dim.2), channel_id=1, replica_groups=mesh['fs_hi'=8,'fs_lo'=2,'rep'=4,'tp_0'=4,'tp_1'=2] {'fs_hi','fs_lo'}, dimensions={0} | all-to-all | bytes 65536 | tf_op jit(solution)/shard_map/all_to_all | solution.py:27
  135.9 0.6 broadcast_in_dim.16
  136.5 7.6 %all-to-all-start.5 = ((f32[8,4,128]{2,1,0:T(4,128)}), f32[8,4,128]{2,1,0:T(4,128)S(1)}, u32[]{:S(2)}, u32[]{:S(2)}) async-start(f32[8,4,128]{2,1,0:T(4,128)} %broadcast_in_dim.16), calls=%async_computation.5 | async-start | bytes 32768 | tf_op jit(solution)/shard_map/all_to_all | solution.py:27
  144.2 4.6 %all-to-all-done.5 = f32[8,4,128]{2,1,0:T(4,128)S(1)} async-done(((f32[8,4,128]{2,1,0:T(4,128)}), f32[8,4,128]{2,1,0:T(4,128)S(1)}, u32[]{:S(2)}, u32[]{:S(2)}) %all-to-all-start.5) | async-done | bytes 16416 | tf_op jit(solution)/shard_map/all_to_all | solution.py:27
  148.9 0.5 fusion.8
  152.1 1.3 fusion.5
  153.5 1.6 %fusion.7 = (bf16[128,256]{1,0:T(8,128)(2,1)}, f32[128,256]{1,0:T(8,128)}, f32[128,256]{1,0:T(8,128)}) fusion(f32[128,256]{1,0:T(8,128)} %param.15, f32[128,256]{1,0:T(8,128)S(1)} %get-tuple-element.25, f32[]{:T(128)} %bitcast.18), kind=kLoop, calls=%fused_computation.18 | loop fusion | flops 98304 | bytes 589828 | tf_op jit(solution)/shard_map/convert_element_type | solution.py:104
  (18 shorter events, 0.1 us)
Async XLA Ops:
  0.6 20.5 %copy-start = (bf16[640,2048]{1,0:T(8,128)(2,1)S(1)}, bf16[640,2048]{1,0:T(8,128)(2,1)}, u32[]{:S(2)}) copy-start(bf16[640,2048]{1,0:T(8,128)(2,1)} %param.11) | copy-start | bytes 7864324
  2.3 29.5 %all-to-all-start = ((f32[16,16,256]{2,1,0:T(8,128)}), f32[16,16,256]{2,1,0:T(8,128)S(1)}, u32[]{:S(2)}, u32[]{:S(2)}) async-start(f32[16,16,256]{2,1,0:T(8,128)} %broadcast_in_dim.6), calls=%async_computation | async-start | bytes 524288 | tf_op jit(solution)/shard_map/all_to_all | solution.py:27
  23.1 10.8 %copy-start.2 = (bf16[1,256,256]{2,1,0:T(8,128)(2,1)S(1)}, bf16[1,256,256]{2,1,0:T(8,128)(2,1)}, u32[]{:S(2)}) copy-start(bf16[1,256,256]{2,1,0:T(8,128)(2,1)} %param.21) | copy-start | bytes 393220
  75.3 33.7 %copy-start.5 = (f32[1,16,256]{2,1,0:T(8,128)S(1)}, f32[1,16,256]{2,1,0:T(8,128)}, u32[]{:S(2)}) copy-start(f32[1,16,256]{2,1,0:T(8,128)} %param.19) | copy-start | bytes 49156
  75.3 39.3 %copy-start.3 = (bf16[256,256]{1,0:T(8,128)(2,1)S(1)}, bf16[256,256]{1,0:T(8,128)(2,1)}, u32[]{:S(2)}) copy-start(bf16[256,256]{1,0:T(8,128)(2,1)} %param.17) | copy-start | bytes 393220
  75.3 39.3 %copy-start.4 = (f32[128,256]{1,0:T(8,128)S(1)}, f32[128,256]{1,0:T(8,128)}, u32[]{:S(2)}) copy-start(f32[128,256]{1,0:T(8,128)} %param.16) | copy-start | bytes 393220
  105.7 8.3 %all-to-all-start.3 = ((f32[4,40,256]{2,1,0:T(8,128)}), f32[4,40,256]{2,1,0:T(8,128)S(1)}, u32[]{:S(2)}, u32[]{:S(2)}) async-start(f32[4,40,256]{2,1,0:T(8,128)} %broadcast_in_dim.7), calls=%async_computation.3 | async-start | bytes 327680 | tf_op jit(solution)/shard_map/all_to_all | solution.py:27
  115.5 39.7 %copy-start.1 = (f32[128,256]{1,0:T(8,128)}, f32[128,256]{1,0:T(8,128)S(1)}, u32[]{:S(2)}) copy-start(f32[128,256]{1,0:T(8,128)S(1)} %get-tuple-element.25) | copy-start | bytes 393220
  136.5 12.3 %all-to-all-start.5 = ((f32[8,4,128]{2,1,0:T(4,128)}), f32[8,4,128]{2,1,0:T(4,128)S(1)}, u32[]{:S(2)}, u32[]{:S(2)}) async-start(f32[8,4,128]{2,1,0:T(4,128)} %broadcast_in_dim.16), calls=%async_computation.5 | async-start | bytes 32768 | tf_op jit(solution)/shard_map/all_to_all | solution.py:27

commit v2 on v1

v2 whole, which is shorter than its diff:
```python
import jax
import jax.numpy as jnp
from jax import lax
from jax.experimental import pallas as pl
from jax.experimental.pallas import tpu as pltpu
from jax.sharding import Mesh
from jax.sharding import PartitionSpec as P

TP = ("tp_0", "tp_1")

BETA = 0.9
LEARN_RATE = 0.02
EPSILON = 1e-06
GROUPS = 4
GRANT = 16 << 20
F32 = jnp.float32
HIGH = lax.Precision.HIGHEST
ALONG_ROWS = (((0,), (0,)), ((), ()))
ALONG_COLUMNS = (((1,), (1,)), ((), ()))


def size_of(axes):
    axes = (axes,) if isinstance(axes, str) else axes
    size = 1
    for axis in axes:
        size *= lax.axis_size(axis)
    return size


def exchange(tiles, axes):
    return lax.all_to_all(tiles, axes, split_axis=0, concat_axis=0, tiled=True)


def whole():
    return pl.BlockSpec(memory_space=pltpu.VMEM)


def on_core(kernel, outs, args, scratch=(), flops=1 << 26):
    moved = sum(a.size * a.dtype.itemsize for a in (*args, *outs))
    single = len(outs) == 1
    return pl.pallas_call(
        kernel,
        out_shape=outs[0] if single else outs,
        in_specs=[whole() for _ in args],
        out_specs=whole() if single else [whole() for _ in outs],
        scratch_shapes=list(scratch),
        compiler_params=pltpu.CompilerParams(vmem_limit_bytes=GRANT),
        cost_estimate=pl.CostEstimate(
            flops=flops, bytes_accessed=moved, transcendentals=0
        ),
    )(*args)


def product_kernel(normed, rec_cot, conv_out, gate_cot, tiles, turned):
    rep, rows, _ = tiles.shape
    group = pl.program_id(0)

    @pl.when(group == 0)
    def _():
        turned[...] = lax.dot_general(
            gate_cot[...], conv_out[...], ALONG_ROWS, preferred_element_type=F32
        )

    part = lax.dot_general(
        normed[...], rec_cot[...], ALONG_ROWS, preferred_element_type=F32
    )
    share = turned.shape[0] // rep
    piece = share // GROUPS
    rec_rows = rows - piece
    owners = rec_rows * rep // 128
    run = rec_rows // owners
    for owner in range(owners):
        for r in range(rep):
            start = (owner * rep + r) * run
            tiles[r, pl.ds(owner * run, run), :] = part[start : start + run]
    for r in range(rep):
        at = pl.multiple_of(r * share + group * piece, piece)
        tiles[r, pl.ds(rec_rows, piece), :] = turned[pl.ds(at, piece), :]


def product(normed, rec_cot, conv_out, gate_cot, rep):
    tokens, width = normed.shape
    block = rec_cot.shape[1]
    rows = (width + block) // rep
    fixed = pl.BlockSpec((tokens, block), lambda g: (0, 0))
    flops = 2 * tokens * block * (width + block)
    return pl.pallas_call(
        product_kernel,
        grid=(GROUPS,),
        in_specs=[
            pl.BlockSpec((tokens, width // GROUPS), lambda g: (0, g)),
            fixed,
            fixed,
            fixed,
        ],
        out_specs=pl.BlockSpec((rep, rows // GROUPS, block), lambda g: (0, g, 0)),
        out_shape=jax.ShapeDtypeStruct((rep, rows, block), F32),
        scratch_shapes=[pltpu.VMEM((block, block), F32)],
        cost_estimate=pl.CostEstimate(
            flops=flops, bytes_accessed=1 << 22, transcendentals=0
        ),
    )(normed, rec_cot, conv_out, gate_cot)


def gather_kernel(arrived, tiles, turned):
    rep = arrived.shape[0]
    fs, run, _ = tiles.shape
    rows = arrived.shape[1] // GROUPS
    piece = turned.shape[0] // GROUPS
    owners = fs // GROUPS
    for g in range(GROUPS):
        total = arrived[0, pl.ds(g * rows, rows), :]
        for r in range(1, rep):
            total += arrived[r, pl.ds(g * rows, rows), :]
        for owner in range(owners):
            tiles[g * owners + owner] = total[owner * run : (owner + 1) * run]
        turned[pl.ds(g * piece, piece), :] = total[owners * run :]


def gather(arrived, fs):
    rep, rows, block = arrived.shape
    share = block // rep
    tiles = jax.ShapeDtypeStruct((fs, (rows - share) // fs, block), F32)
    turned = jax.ShapeDtypeStruct((share, block), F32)
    return on_core(gather_kernel, (tiles, turned), (arrived,))


def middle_kernel(rec_tiles, gates, left, tiles):
    fs, run, block = rec_tiles.shape
    half = block // 2
    depth = left.shape[1] // 2
    turned = gates[...]
    blank = jnp.zeros_like(turned)
    done = None
    for q in range(2):
        rows_q = left[:, pl.ds(q * depth, depth), :].reshape(fs * depth, block)
        wide = [blank] * q + [turned]
        wide += [blank] * (half // turned.shape[0] - len(wide))
        term = lax.dot_general(
            rows_q,
            jnp.concatenate(wide, axis=0),
            ALONG_COLUMNS,
            precision=HIGH,
            preferred_element_type=F32,
        )
        done = term if done is None else done + term
    for f in range(fs):
        row, side = f // 2 * depth, f % 2 * half
        tiles[f, pl.ds(0, run), :] = rec_tiles[f]
        tiles[f, pl.ds(run, depth), pl.ds(0, half)] = turned[
            row : row + depth, side : side + half
        ]
        tiles[f, pl.ds(run, depth), pl.ds(half, half)] = done[
            f * depth : (f + 1) * depth
        ]


def middle(rec_tiles, gates, left):
    fs, run, block = rec_tiles.shape
    out = jax.ShapeDtypeStruct((fs, run + left.shape[1] // 2, block), F32)
    return on_core(middle_kernel, (out,), (rec_tiles, gates, left), flops=1 << 30)


def fold_kernel(tiles, copies):
    total = tiles[0]
    for i in range(1, tiles.shape[0]):
        total += tiles[i]
    for i in range(copies.shape[0]):
        copies[i] = total


def fold(tiles, count):
    out = jax.ShapeDtypeStruct((count, *tiles.shape[1:]), F32)
    return on_core(fold_kernel, (out,), (tiles,))


def decay_kernel(rec_moment, gate_moment, rec_out, gate_out):
    rec_out[...] = BETA * rec_moment[...]
    gate_out[...] = BETA * gate_moment[...]


def square_sum(value):
    return jnp.sum(jnp.sum(value * value, axis=0, keepdims=True), axis=1, keepdims=True)


def moments_kernel(
    full,
    rec_right,
    gate_right,
    rec_moment,
    gate_moment,
    rec_out,
    gate_out,
    sums,
):
    rep, _, block = full.shape
    n_rec = rec_moment.shape[0] // rep
    half, share = block // 2, block // rep
    depth = full.shape[1] - n_rec
    rec_grad = full[:, pl.ds(0, n_rec), :].reshape(rep * n_rec, block)
    rec_pre = jnp.dot(
        rec_grad, rec_right[...].astype(F32), precision=HIGH, preferred_element_type=F32
    )
    rec_new = rec_moment[...] + rec_pre
    rec_out[...] = rec_new

    gate_grad = full[:, pl.ds(n_rec, depth), pl.ds(0, half)]
    done = jnp.concatenate(
        [full[r, pl.ds(n_rec, depth), pl.ds(half, half)] for r in range(rep)], axis=1
    )
    right = gate_right[...].astype(F32)
    blank = jnp.zeros((share, block), F32)
    parts = []
    for q in range(2):
        wide = []
        for r in range(rep):
            mine = right[r * share : (r + 1) * share]
            wide += [blank] * q + [mine] + [blank] * (1 - q)
        parts.append(
            jnp.dot(
                done,
                jnp.concatenate(wide, axis=0),
                precision=HIGH,
                preferred_element_type=F32,
            )
        )
    gate_new = gate_moment[...] + jnp.concatenate(parts, axis=0)
    gate_out[...] = gate_new

    row = lax.broadcasted_iota(jnp.int32, sums.shape[1:], 0)
    tile = jnp.zeros(sums.shape[1:], F32)
    squares = (
        square_sum(rec_grad),
        square_sum(rec_new),
        square_sum(gate_grad.reshape(rep * depth, half)),
        square_sum(gate_new),
    )
    for i, value in enumerate(squares):
        tile = jnp.where(row == i, value, tile)
    for i in range(sums.shape[0]):
        sums[i] = tile


def update_kernel(
    sums,
    rec_weight,
    rec_moment,
    gate_weight,
    gate_moment,
    rec_new,
    rec_step,
    rec_copy,
    gate_new,
    gate_step,
    gate_copy,
):
    total = sums[0]
    for i in range(1, sums.shape[0]):
        total += sums[i]
    places = (
        (rec_weight, rec_moment, rec_new, rec_step, rec_copy),
        (gate_weight, gate_moment, gate_new, gate_step, gate_copy),
    )
    for i, (weight, moment, new, step, copy) in enumerate(places):
        scale = jnp.sqrt(total[2 * i : 2 * i + 1]) / jnp.sqrt(
            total[2 * i + 1 : 2 * i + 2] + EPSILON
        )
        scale = jnp.concatenate([LEARN_RATE * scale] * 2, axis=1)
        taken = scale * moment[...]
        value = weight[...] - taken
        step[...] = taken
        new[...] = value
        copy[...] = value.astype(jnp.bfloat16)


def shards(
    normed,
    rec_cot,
    conv_out,
    gate_cot,
    rec_weight,
    rec_moment,
    rec_right,
    gate_weight,
    gate_moment,
    gate_left,
    gate_right,
):
    fs, rep = lax.axis_size("fs"), lax.axis_size("rep")
    like = lambda value, kind=F32: jax.ShapeDtypeStruct(value.shape, kind)
    gate_weight, gate_moment = gate_weight[0], gate_moment[0]

    with jax.named_scope("left"):
        left = gate_left[0].astype(F32)
        left = lax.all_gather(left, "fs")
    with jax.named_scope("product"):
        tiles = product(normed, rec_cot, conv_out, gate_cot, rep)
    with jax.named_scope("near"):
        arrived = exchange(tiles, "rep")
    with jax.named_scope("decay"):
        rec_moment, gate_moment = on_core(
            decay_kernel,
            (like(rec_moment), like(gate_moment)),
            (rec_moment, gate_moment),
        )
    with jax.named_scope("gather"):
        rec_tiles, gates = gather(arrived, fs)
    with jax.named_scope("middle"):
        tiles = middle(rec_tiles, gates, left)
    with jax.named_scope("far"):
        arrived = exchange(tiles, "fs")
    with jax.named_scope("fold"):
        tiles = fold(arrived, rep)
    with jax.named_scope("share"):
        full = exchange(tiles, "rep")
    with jax.named_scope("moments"):
        rec_moment_new, gate_moment_new, sums = on_core(
            moments_kernel,
            (
                like(rec_moment),
                like(gate_moment),
                jax.ShapeDtypeStruct((fs, 8, 128), F32),
            ),
            (full, rec_right, gate_right[0], rec_moment, gate_moment),
        )
    with jax.named_scope("sums"):
        sums = fold(exchange(sums, "fs"), size_of(TP))
        sums = exchange(sums, TP)
    with jax.named_scope("update"):
        bf16 = jnp.bfloat16
        rec_new, rec_step, rec_copy, gate_new, gate_step, gate_copy = on_core(
            update_kernel,
            (
                like(rec_weight),
                like(rec_weight),
                like(rec_weight, bf16),
                like(gate_weight),
                like(gate_weight),
                like(gate_weight, bf16),
            ),
            (sums, rec_weight, rec_moment_new, gate_weight, gate_moment_new),
        )
    return (
        rec_new,
        rec_moment_new,
        rec_step,
        rec_copy,
        gate_new[None],
        gate_moment_new[None],
        gate_step[None],
        gate_copy[None],
    )


def solution(mesh):
    fs, rep, tp = (mesh.shape[name] for name in ("fs", "rep", "tp"))
    split = Mesh(
        mesh.devices.reshape(fs, rep, tp // 2, 2),
        ("fs", "rep", *TP),
    )
    tokens = ("fs", "rep")
    placed = (
        P(tokens, None),
        P(tokens, TP),
        P(tokens, TP),
        P(tokens, TP),
        P("fs", TP),
        P("fs", TP),
        P(TP, None),
        P(TP, "fs", None),
        P(TP, "fs", None),
        P(TP, "fs", None),
        P(TP, None, None),
    )

    return jax.shard_map(
        shards,
        mesh=split,
        in_specs=placed,
        out_specs=(P("fs", TP),) * 4 + (P(TP, "fs", None),) * 4,
        check_vma=False,
    )
```

time: 156 us -> 133 us (0.85)
  blocking collectives: 83.7 us -> 108 us
  starting transfers between devices: 26.7 us -> 8.47 us
  waiting for transfers between devices: 16.7 us -> 4.93 us
  other arithmetic: 11.7 us -> 0.01 us
  Pallas kernels: 0 us -> 8.61 us
  matrix products: 5.72 us -> 0 us
  local copies, waits for them, and re-layouts: 7.03 us -> 1.66 us
  between operations: 3.53 us -> 0.74 us
    all_gather x0 -> x1, blocking collectives: none -> 31.4 us  [shards(): left = lax.all_gather(left, 'fs')]
    all_to_all x3 -> x2, starting transfers between devices: 26.7 us -> 8.47 us  [exchange(): return lax.all_to_all(tiles, axes, split_axis=0, concat_axis=0, tiled=True)]
    all_to_all x3 -> x2, waiting for transfers between devices: 16.7 us -> 4.93 us  [exchange(): return lax.all_to_all(tiles, axes, split_axis=0, concat_axis=0, tiled=True)]
    pallas_call x0 -> x8, Pallas kernels: none -> 8.61 us  [the longest x1 5.4 us: product(): pl.pallas_call(product_kernel, grid=(GROUPS,), in_specs=[pl.BlockSpec((to...]
    all_to_all x3, blocking collectives: 83.7 us -> 76.2 us  [exchange(): return lax.all_to_all(tiles, axes, split_axis=0, concat_axis=0, tiled=True)]
    dot_general x5 -> x0, matrix products: 5.72 us -> none  [the longest x1 2 us: shards(): lax.dot_general(normed, rec_cot, contract, preferred_element_type=F32)]
    convert_element_type x3 -> x1, other arithmetic: 3.83 us -> 0.01 us  [shards(): left = gate_left[0].astype(F32)]
    reduce_sum x6 -> x0, other arithmetic: 3.3 us -> none  [the longest x1 1.99 us: shards(): near = exchange(tiles, NEAR).sum(axis=0)]
  transfers between devices with their start and end apart: 3 -> 2, of which waited for: 3 -> 1; matrix products, arithmetic and copies ran while one was open for 4% -> 0% of each run, Pallas kernels for 0% -> 0%
where the time goes in v2:
time: 133 us; the launch traced here: 132 us
  blocking collectives  108 us (81%)
  Pallas kernels  8.61 us (6%)
  starting transfers between devices  8.47 us (6%)
  waiting for transfers between devices  4.93 us (4%)
  local copies, waits for them, and re-layouts  1.66 us (1%)
    all_to_all x3, blocking collectives, exchange(): return lax.all_to_all(tiles, axes, split_axis=0, concat_axis=0, tiled=True)  76.2 us
    all_gather x1, blocking collectives, shards(): left = lax.all_gather(left, 'fs')  31.4 us
    all_to_all x2, starting transfers between devices, exchange(): return lax.all_to_all(tiles, axes, split_axis=0, concat_axis=0, tiled=True)  8.47 us
    pallas_call x1, Pallas kernels, product(): pl.pallas_call(product_kernel, grid=(GROUPS,), in_specs=[pl.BlockSpec((to...  5.4 us
    all_to_all x2, waiting for transfers between devices, exchange(): return lax.all_to_all(tiles, axes, split_axis=0, concat_axis=0, tiled=True)  4.93 us
    pallas_call x7, Pallas kernels, on_core(): pl.pallas_call(kernel, out_shape=outs[0] if single else outs, in_specs=[w...  3.21 us
  transfers between devices with their start and end apart: 2, of which 1 were waited for; matrix products, arithmetic and copies ran while one was open for 0% of the time, Pallas kernels for 0%

profile of v2, /device:TPU:1, one launch (start us, length us, event | category | flops | bytes accessed | tf_op | source)
XLA Modules:
  0.0 132.1 jit_solution(2294047462023251719)
XLA Ops:
  0.6 5.4 %product.1 = f32[4,576,256]{2,1,0:T(8,128)} custom-call(bf16[640,2048]{1,0:T(8,128)(2,1)} %normed.1, bf16[640,256]{1,0:T(8,128)(2,1)} %rec_cot.1, bf16[640,256]{1,0:T(8,128)(2,1)} %conv_out.1, bf16[640,256]{1,0:T(8,128)(2,1)} %gate_cot.1), custom_call_target="tpu_custom_call" | custom-call | flops 754974720 | bytes 4194304 | tf_op jit(solution)/shard_map/product/pallas_call | solution.py:87
  6.0 0.0 copy-start.8
  6.0 5.1 %all-to-all-start = ((f32[4,576,256]{2,1,0:T(8,128)}), f32[4,576,256]{2,1,0:T(8,128)S(1)}, u32[]{:S(2)}, u32[]{:S(2)}) async-start(f32[4,576,256]{2,1,0:T(8,128)} %product.1), calls=%async_computation | async-start | bytes 4718592 | tf_op jit(solution)/shard_map/near/all_to_all | solution.py:31
  11.2 0.0 copy-done.8
  11.2 31.4 %all_gather.4.left = f32[16,16,256]{2,1,0:T(8,128)S(1)} all-gather(f32[1,16,256]{2,1,0:T(8,128)S(1)} %convert_element_type.4), channel_id=1, replica_groups=mesh['fs'=16,'rep'=4,'tp_0'=4,'tp_1'=2] {'fs'}, dimensions={0}, use_global_device_ids=true | all-gather | bytes 278528 | tf_op jit(solution)/shard_map/left/all_gather | solution.py:295
  42.6 0.0 all-to-all-done.arrived
  42.6 0.1 gather.1
  42.7 0.0 copy-start.6
  42.7 0.0 copy-start.7
  42.8 0.0 copy-start.2
  42.8 0.0 copy-start.3
  42.8 0.4 middle.1
  43.1 0.0 copy-start
  43.1 0.0 copy-start.4
  43.2 45.5 %all_to_all.25.tiles = f32[16,40,256]{2,1,0:T(8,128)S(1)} all-to-all(f32[16,40,256]{2,1,0:T(8,128)S(1)} %middle.1), channel_id=1, replica_groups=mesh['fs'=16,'rep'=4,'tp_0'=4,'tp_1'=2] {'fs'}, dimensions={0} | all-to-all | bytes 1310720 | tf_op jit(solution)/shard_map/far/all_to_all | solution.py:31
  88.7 0.7 fold.1
  89.4 3.3 %all-to-all-start.2 = ((f32[4,40,256]{2,1,0:T(8,128)}), f32[4,40,256]{2,1,0:T(8,128)S(1)}, u32[]{:S(2)}, u32[]{:S(2)}) async-start(f32[4,40,256]{2,1,0:T(8,128)} %fold.1), calls=%async_computation.2 | async-start | bytes 327680 | tf_op jit(solution)/shard_map/share/all_to_all | solution.py:31
  92.8 0.0 copy-done.6
  92.8 0.0 copy-done.7
  92.8 4.9 %all-to-all-done.2.full = f32[4,40,256]{2,1,0:T(8,128)S(1)} async-done(((f32[4,40,256]{2,1,0:T(8,128)}), f32[4,40,256]{2,1,0:T(8,128)S(1)}, u32[]{:S(2)}, u32[]{:S(2)}) %all-to-all-start.2) | async-done | bytes 163872 | tf_op jit(solution)/shard_map/share/all_to_all | solution.py:31
  97.7 0.0 copy-done.2
  97.7 0.0 copy-done.3
  97.7 1.2 moments.1
  99.0 18.3 %all_to_all.26.tiles = f32[16,8,128]{2,1,0:T(8,128)S(1)} all-to-all(f32[16,8,128]{2,1,0:T(8,128)S(1)} %get-tuple-element.25), channel_id=1, replica_groups=mesh['fs'=16,'rep'=4,'tp_0'=4,'tp_1'=2] {'fs'}, dimensions={0} | all-to-all | bytes 131072 | tf_op jit(solution)/shard_map/sums/all_to_all | solution.py:31
  117.3 12.4 %all_to_all.27.sums = f32[8,8,128]{2,1,0:T(8,128)S(1)} all-to-all(f32[8,8,128]{2,1,0:T(8,128)S(1)} %sums.1), channel_id=1, replica_groups=mesh['fs'=16,'rep'=4,'tp_0'=4,'tp_1'=2] {'tp_0','tp_1'}, dimensions={0} | all-to-all | bytes 65536 | tf_op jit(solution)/shard_map/sums/all_to_all | solution.py:31
  129.7 0.0 copy-done
  129.7 0.0 copy-done.4
  129.7 0.0 copy-start.1
  129.7 0.9 copy-done.1
  130.6 0.0 copy-start.5
  130.6 0.7 copy-done.5
  131.3 0.8 update.1
  (3 shorter events, 0.0 us)
Async XLA Ops:
  6.0 5.1 %copy-start.8 = (bf16[1,16,256]{2,1,0:T(8,128)(2,1)S(1)}, bf16[1,16,256]{2,1,0:T(8,128)(2,1)}, u32[]{:S(2)}) copy-start(bf16[1,16,256]{2,1,0:T(8,128)(2,1)} %param.20) | copy-start | bytes 24580
  6.0 36.6 %all-to-all-start = ((f32[4,576,256]{2,1,0:T(8,128)}), f32[4,576,256]{2,1,0:T(8,128)S(1)}, u32[]{:S(2)}, u32[]{:S(2)}) async-start(f32[4,576,256]{2,1,0:T(8,128)} %product.1), calls=%async_computation | async-start | bytes 4718592 | tf_op jit(solution)/shard_map/near/all_to_all | solution.py:31
  42.7 50.0 %copy-start.6 = (f32[128,256]{1,0:T(8,128)S(1)}, f32[128,256]{1,0:T(8,128)}, u32[]{:S(2)}) copy-start(f32[128,256]{1,0:T(8,128)} %rec_moment.1) | copy-start | bytes 393220
  42.7 50.0 %copy-start.7 = (f32[1,16,256]{2,1,0:T(8,128)S(1)}, f32[1,16,256]{2,1,0:T(8,128)}, u32[]{:S(2)}) copy-start(f32[1,16,256]{2,1,0:T(8,128)} %param.19) | copy-start | bytes 49156
  42.8 55.0 %copy-start.2 = (bf16[256,256]{1,0:T(8,128)(2,1)S(1)}, bf16[256,256]{1,0:T(8,128)(2,1)}, u32[]{:S(2)}) copy-start(bf16[256,256]{1,0:T(8,128)(2,1)} %rec_right.1) | copy-start | bytes 393220
  42.8 55.0 %copy-start.3 = (bf16[1,256,256]{2,1,0:T(8,128)(2,1)S(1)}, bf16[1,256,256]{2,1,0:T(8,128)(2,1)}, u32[]{:S(2)}) copy-start(bf16[1,256,256]{2,1,0:T(8,128)(2,1)} %param.21) | copy-start | bytes 393220
  43.1 86.5 %copy-start = (f32[128,256]{1,0:T(8,128)S(1)}, f32[128,256]{1,0:T(8,128)}, u32[]{:S(2)}) copy-start(f32[128,256]{1,0:T(8,128)} %rec_weight.1) | copy-start | bytes 393220
  43.1 86.5 %copy-start.4 = (f32[1,16,256]{2,1,0:T(8,128)S(1)}, f32[1,16,256]{2,1,0:T(8,128)}, u32[]{:S(2)}) copy-start(f32[1,16,256]{2,1,0:T(8,128)} %param.18) | copy-start | bytes 49156
  89.4 8.3 %all-to-all-start.2 = ((f32[4,40,256]{2,1,0:T(8,128)}), f32[4,40,256]{2,1,0:T(8,128)S(1)}, u32[]{:S(2)}, u32[]{:S(2)}) async-start(f32[4,40,256]{2,1,0:T(8,128)} %fold.1), calls=%async_computation.2 | async-start | bytes 327680 | tf_op jit(solution)/shard_map/share/all_to_all | solution.py:31
  129.7 0.9 copy-start.1
  130.6 0.7 copy-start.5

commit v3 on v2

v3 whole, which is shorter than its diff:
```python
import jax
import jax.numpy as jnp
from jax import lax
from jax.experimental import pallas as pl
from jax.experimental.pallas import tpu as pltpu
from jax.sharding import Mesh
from jax.sharding import PartitionSpec as P

FS = ("fs_hi", "fs_lo")
TP = ("tp_0", "tp_1")

BETA = 0.9
LEARN_RATE = 0.02
EPSILON = 1e-06
GROUPS = 4
GRANT = 16 << 20
F32 = jnp.float32
HIGH = lax.Precision.HIGHEST
ALONG_ROWS = (((0,), (0,)), ((), ()))
ALONG_COLUMNS = (((1,), (1,)), ((), ()))


def size_of(axes):
    axes = (axes,) if isinstance(axes, str) else axes
    size = 1
    for axis in axes:
        size *= lax.axis_size(axis)
    return size


def exchange(tiles, axes):
    return lax.all_to_all(tiles, axes, split_axis=0, concat_axis=0, tiled=True)


def whole():
    return pl.BlockSpec(memory_space=pltpu.VMEM)


def on_core(kernel, outs, args, scratch=(), flops=1 << 26):
    moved = sum(a.size * a.dtype.itemsize for a in (*args, *outs))
    single = len(outs) == 1
    return pl.pallas_call(
        kernel,
        out_shape=outs[0] if single else outs,
        in_specs=[whole() for _ in args],
        out_specs=whole() if single else [whole() for _ in outs],
        scratch_shapes=list(scratch),
        compiler_params=pltpu.CompilerParams(vmem_limit_bytes=GRANT),
        cost_estimate=pl.CostEstimate(
            flops=flops, bytes_accessed=moved, transcendentals=0
        ),
    )(*args)


def product_kernel(normed, rec_cot, conv_out, gate_cot, right, tiles, turned):
    rep, rows, _ = tiles.shape
    group = pl.program_id(0)

    @pl.when(group == 0)
    def _():
        grad = lax.dot_general(
            gate_cot[...], conv_out[...], ALONG_ROWS, preferred_element_type=F32
        )
        turned[0] = grad
        turned[1] = lax.dot_general(
            right[...].astype(F32),
            grad,
            ALONG_ROWS,
            precision=HIGH,
            preferred_element_type=F32,
        )

    part = lax.dot_general(
        normed[...], rec_cot[...], ALONG_ROWS, preferred_element_type=F32
    )
    share = turned.shape[1] // rep
    piece = share // GROUPS
    rec_rows = rows - 2 * piece
    run = 128 // rep
    for owner in range(rec_rows // run):
        for r in range(rep):
            start = (owner * rep + r) * run
            tiles[r, pl.ds(owner * run, run), :] = part[start : start + run]
    for r in range(rep):
        at = pl.multiple_of(r * share + group * piece, piece)
        for i in range(2):
            tiles[r, pl.ds(rec_rows + i * piece, piece), :] = turned[
                i, pl.ds(at, piece), :
            ]


def product(normed, rec_cot, conv_out, gate_cot, right, rep):
    tokens, width = normed.shape
    block = rec_cot.shape[1]
    rows = (width + 2 * block) // rep
    fixed = pl.BlockSpec((tokens, block), lambda g: (0, 0))
    flops = 2 * tokens * block * (width + block)
    return pl.pallas_call(
        product_kernel,
        grid=(GROUPS,),
        in_specs=[
            pl.BlockSpec((tokens, width // GROUPS), lambda g: (0, g)),
            fixed,
            fixed,
            fixed,
            pl.BlockSpec((block, block), lambda g: (0, 0)),
        ],
        out_specs=pl.BlockSpec((rep, rows // GROUPS, block), lambda g: (0, g, 0)),
        out_shape=jax.ShapeDtypeStruct((rep, rows, block), F32),
        scratch_shapes=[pltpu.VMEM((2, block, block), F32)],
        cost_estimate=pl.CostEstimate(
            flops=flops, bytes_accessed=1 << 22, transcendentals=0
        ),
    )(normed, rec_cot, conv_out, gate_cot, right)


def middle_kernel(arrived, left, tiles):
    rep = arrived.shape[0]
    fs, _, block = tiles.shape
    rows = arrived.shape[1] // GROUPS
    share = block // rep
    piece = share // GROUPS
    rec_rows = rows - 2 * piece
    owners = fs // GROUPS
    run = rec_rows // owners
    half = block // 2
    grads, rights = [], []
    for g in range(GROUPS):
        total = arrived[0, pl.ds(g * rows, rows), :]
        for r in range(1, rep):
            total += arrived[r, pl.ds(g * rows, rows), :]
        for owner in range(owners):
            tiles[g * owners + owner, pl.ds(0, run), :] = total[
                owner * run : (owner + 1) * run
            ]
        grads.append(total[rec_rows : rec_rows + piece])
        rights.append(total[rec_rows + piece :])
    turned = jnp.concatenate(grads, axis=0)
    right_done = jnp.concatenate(rights, axis=0)
    blank = jnp.zeros_like(right_done)
    depth = left.shape[1] // 2
    done = None
    for q in range(2):
        rows_q = left[:, pl.ds(q * depth, depth), :].reshape(fs * depth, block)
        wide = [blank] * q + [right_done] + [blank] * (1 - q)
        term = lax.dot_general(
            rows_q,
            jnp.concatenate(wide, axis=0),
            ALONG_COLUMNS,
            precision=HIGH,
            preferred_element_type=F32,
        )
        done = term if done is None else done + term
    for f in range(fs):
        row, side = f // 2 * depth, f % 2 * half
        tiles[f, pl.ds(run, depth), pl.ds(0, half)] = turned[
            row : row + depth, side : side + half
        ]
        tiles[f, pl.ds(run, depth), pl.ds(half, half)] = done[
            f * depth : (f + 1) * depth
        ]


def middle(arrived, left):
    fs, own_rows, block = left.shape
    rec_rows = arrived.shape[1] - 2 * block // arrived.shape[0]
    out = jax.ShapeDtypeStruct((fs, rec_rows // fs + own_rows // 2, block), F32)
    return on_core(middle_kernel, (out,), (arrived, left), flops=1 << 30)


def fold_kernel(tiles, after, copies):
    total = tiles[0]
    for i in range(1, tiles.shape[0]):
        total += tiles[i]
    for i in range(copies.shape[0]):
        copies[i] = total


def fold(tiles, count, after):
    out = jax.ShapeDtypeStruct((count, *tiles.shape[1:]), F32)
    return on_core(fold_kernel, (out,), (tiles, after))


def square_sum(value):
    return jnp.sum(jnp.sum(value * value, axis=0, keepdims=True), axis=1, keepdims=True)


def placing(block, share, q, r):
    lane = lax.broadcasted_iota(jnp.int32, (2 * share, block), 0) - q * share
    column = lax.broadcasted_iota(jnp.int32, (2 * share, block), 1) - r * share
    inside = (lane >= 0) & (lane < share)
    return jnp.where(inside & (lane == column), 1.0, 0.0).astype(F32)


def settle_kernel(arrived, rec_right, rec_moment, gate_moment, mine, sums):
    _, rows, block = arrived.shape
    rep = lax.axis_size("rep")
    r = lax.axis_index("rep")
    run = rec_moment.shape[0] // rep
    depth = rows - run
    half, share = block // 2, block // rep
    total = arrived[0]
    for i in range(1, arrived.shape[0]):
        total += arrived[i]
    rec_grad = total[:run]
    rec_pre = jnp.dot(
        rec_grad, rec_right[...].astype(F32), precision=HIGH, preferred_element_type=F32
    )
    start = pl.multiple_of(r * run, run)
    rec_new = BETA * rec_moment[pl.ds(start, run), :] + rec_pre
    mine[pl.ds(0, run), :] = rec_new

    gate_grad = total[run:, :half]
    packed = None
    for q in range(2):
        term = lax.dot_general(
            gate_moment[pl.ds(q * depth, depth), :],
            placing(block, share, q, r),
            ALONG_COLUMNS,
            precision=HIGH,
            preferred_element_type=F32,
        )
        packed = term if packed is None else packed + term
    gate_new = BETA * packed + total[run:, half:]
    mine[pl.ds(run, depth), pl.ds(0, half)] = gate_new
    mine[pl.ds(run, depth), pl.ds(half, half)] = gate_new

    row = lax.broadcasted_iota(jnp.int32, sums.shape[1:], 0)
    tile = jnp.zeros(sums.shape[1:], F32)
    for i, value in enumerate((rec_grad, rec_new, gate_grad, gate_new)):
        tile = jnp.where(row == i, square_sum(value), tile)
    for i in range(sums.shape[0]):
        sums[i] = tile


def update_kernel(
    sums,
    full,
    rec_weight,
    gate_weight,
    rec_new,
    rec_moment,
    rec_step,
    rec_copy,
    gate_new,
    gate_moment,
    gate_step,
    gate_copy,
):
    rep, rows, block = full.shape
    run = rec_weight.shape[0] // rep
    depth = rows - run
    half, share = block // 2, block // rep
    rec_value = full[:, pl.ds(0, run), :].reshape(rep * run, block)
    parts = []
    for q in range(2):
        part = None
        for r in range(rep):
            term = jnp.dot(
                full[r, pl.ds(run, depth), pl.ds(0, half)],
                placing(block, share, q, r),
                precision=HIGH,
                preferred_element_type=F32,
            )
            part = term if part is None else part + term
        parts.append(part)
    gate_value = jnp.concatenate(parts, axis=0)

    total = sums[0]
    for i in range(1, sums.shape[0]):
        total += sums[i]
    places = (
        (rec_value, rec_weight, rec_new, rec_moment, rec_step, rec_copy),
        (gate_value, gate_weight, gate_new, gate_moment, gate_step, gate_copy),
    )
    for i, (value, weight, new, moment, step, copy) in enumerate(places):
        scale = jnp.sqrt(total[2 * i : 2 * i + 1]) / jnp.sqrt(
            total[2 * i + 1 : 2 * i + 2] + EPSILON
        )
        scale = jnp.concatenate([LEARN_RATE * scale] * 2, axis=1)
        taken = scale * value
        result = weight[...] - taken
        moment[...] = value
        step[...] = taken
        new[...] = result
        copy[...] = result.astype(jnp.bfloat16)


def shards(
    normed,
    rec_cot,
    conv_out,
    gate_cot,
    rec_weight,
    rec_moment,
    rec_right,
    gate_weight,
    gate_moment,
    gate_left,
    gate_right,
):
    fs, rep = size_of(FS), lax.axis_size("rep")
    like = lambda value, kind=F32: jax.ShapeDtypeStruct(value.shape, kind)
    gate_weight, gate_moment = gate_weight[0], gate_moment[0]
    own_rows, block = gate_weight.shape

    with jax.named_scope("product"):
        tiles = product(normed, rec_cot, conv_out, gate_cot, gate_right[0], rep)
    with jax.named_scope("near"):
        arrived = exchange(tiles, "rep")
    with jax.named_scope("left"):
        left = lax.all_gather(gate_left[0].astype(F32), "fs_lo")
        left = lax.all_gather(left, "fs_hi").reshape(fs, own_rows, block)
    with jax.named_scope("middle"):
        tiles = middle(arrived, left)
    with jax.named_scope("far"):
        arrived = exchange(tiles, FS)
    with jax.named_scope("settle"):
        mine, sums = on_core(
            settle_kernel,
            (
                jax.ShapeDtypeStruct(arrived.shape[1:], F32),
                jax.ShapeDtypeStruct((fs, 8, 128), F32),
            ),
            (arrived, rec_right, rec_moment, gate_moment),
        )
    with jax.named_scope("share"):
        full = lax.all_gather(mine, "rep")
    with jax.named_scope("sums"):
        sums = fold(exchange(sums, FS), rep * size_of(TP), full)
        sums = exchange(sums, ("rep", *TP))
    with jax.named_scope("update"):
        bf16 = jnp.bfloat16
        (
            rec_new,
            rec_moment_new,
            rec_step,
            rec_copy,
            gate_new,
            gate_moment_new,
            gate_step,
            gate_copy,
        ) = on_core(
            update_kernel,
            (
                like(rec_weight),
                like(rec_weight),
                like(rec_weight),
                like(rec_weight, bf16),
                like(gate_weight),
                like(gate_weight),
                like(gate_weight),
                like(gate_weight, bf16),
            ),
            (sums, full, rec_weight, gate_weight),
        )
    return (
        rec_new,
        rec_moment_new,
        rec_step,
        rec_copy,
        gate_new[None],
        gate_moment_new[None],
        gate_step[None],
        gate_copy[None],
    )


def solution(mesh):
    fs, rep, tp = (mesh.shape[name] for name in ("fs", "rep", "tp"))
    split = Mesh(
        mesh.devices.reshape(fs // 4, 4, rep, tp // 2, 2),
        (*FS, "rep", *TP),
    )
    tokens = (*FS, "rep")
    placed = (
        P(tokens, None),
        P(tokens, TP),
        P(tokens, TP),
        P(tokens, TP),
        P(FS, TP),
        P(FS, TP),
        P(TP, None),
        P(TP, FS, None),
        P(TP, FS, None),
        P(TP, FS, None),
        P(TP, None, None),
    )

    return jax.shard_map(
        shards,
        mesh=split,
        in_specs=placed,
        out_specs=(P(FS, TP),) * 4 + (P(TP, FS, None),) * 4,
        check_vma=False,
    )
```

time: 133 us -> 128 us (0.962)
  starting transfers between devices: 8.47 us -> 14.8 us
  blocking collectives: 108 us -> 102 us
  waiting for transfers between devices: 4.93 us -> 1.81 us
  local copies, waits for them, and re-layouts: 1.66 us -> 0.02 us
    all_to_all x3 -> x2, blocking collectives: 76.2 us -> 54.7 us  [exchange(): return lax.all_to_all(tiles, axes, split_axis=0, concat_axis=0, tiled=True)]
    all_gather x1 -> x3, blocking collectives: 31.4 us -> 46.9 us  [the longest x1 25.8 us: shards(): left = lax.all_gather(left, 'fs_hi').reshape(fs, own_rows, block)]
    all_to_all x2, starting transfers between devices: 8.47 us -> 14.8 us  [exchange(): return lax.all_to_all(tiles, axes, split_axis=0, concat_axis=0, tiled=True)]
    all_to_all x2, waiting for transfers between devices: 4.93 us -> 1.81 us  [exchange(): return lax.all_to_all(tiles, axes, split_axis=0, concat_axis=0, tiled=True)]
    unnamed x18 -> x12, local copies, waits for them, and re-layouts: 1.66 us -> 0.02 us
    pallas_call x7 -> x4, Pallas kernels: 3.21 us -> 2.61 us  [on_core(): pl.pallas_call(kernel, out_shape=outs[0] if single else outs, in_specs=[w...]
where the time goes in v3:
time: 128 us; the launch traced here: 127 us
  blocking collectives  102 us (80%)
  starting transfers between devices  14.8 us (12%)
  Pallas kernels  8.54 us (7%)
  waiting for transfers between devices  1.81 us (1%)
    all_to_all x2, blocking collectives, exchange(): return lax.all_to_all(tiles, axes, split_axis=0, concat_axis=0, tiled=True)  54.7 us
    all_gather x1, blocking collectives, shards(): left = lax.all_gather(left, 'fs_hi').reshape(fs, own_rows, block)  25.8 us
    all_to_all x2, starting transfers between devices, exchange(): return lax.all_to_all(tiles, axes, split_axis=0, concat_axis=0, tiled=True)  14.8 us
    all_gather x1, blocking collectives, shards(): left = lax.all_gather(gate_left[0].astype(F32), 'fs_lo')  11.3 us
    all_gather x1, blocking collectives, shards(): full = lax.all_gather(mine, 'rep')  9.76 us
    pallas_call x1, Pallas kernels, product(): pl.pallas_call(product_kernel, grid=(GROUPS,), in_specs=[pl.BlockSpec((to...  5.93 us
    pallas_call x4, Pallas kernels, on_core(): pl.pallas_call(kernel, out_shape=outs[0] if single else outs, in_specs=[w...  2.61 us
  transfers between devices with their start and end apart: 2, of which 1 were waited for; matrix products, arithmetic and copies ran while one was open for 0% of the time, Pallas kernels for 0%

profile of v3, /device:TPU:1, one launch (start us, length us, event | category | flops | bytes accessed | tf_op | source)
XLA Modules:
  0.0 127.5 jit_solution(5051261720933641953)
XLA Ops:
  0.6 5.9 %product.1 = f32[4,640,256]{2,1,0:T(8,128)} custom-call(bf16[640,2048]{1,0:T(8,128)(2,1)} %normed.1, bf16[640,256]{1,0:T(8,128)(2,1)} %rec_cot.1, bf16[640,256]{1,0:T(8,128)(2,1)} %conv_out.1, bf16[640,256]{1,0:T(8,128)(2,1)} %gate_cot.1, bf16[256,256]{1,0:T(8,128)(2,1)} %bitcast.12), custom_call_target="tpu_custom_call" | custom-call | flops 754974720 | bytes 4194304 | tf_op jit(solution)/shard_map/product/pallas_call | solution.py:98
  6.6 0.0 copy-start.5
  6.6 5.1 %all-to-all-start = ((f32[4,640,256]{2,1,0:T(8,128)}), f32[4,640,256]{2,1,0:T(8,128)S(1)}, u32[]{:S(2)}, u32[]{:S(2)}) async-start(f32[4,640,256]{2,1,0:T(8,128)} %product.1), calls=%async_computation | async-start | bytes 5242880 | tf_op jit(solution)/shard_map/near/all_to_all | solution.py:32
  11.7 0.0 copy-done.5
  11.7 11.3 %all_gather.16 = f32[4,16,256]{2,1,0:T(8,128)S(1)} all-gather(f32[1,16,256]{2,1,0:T(8,128)S(1)} %convert_element_type.4), channel_id=1, replica_groups=mesh['fs_hi'=4,'fs_lo'=4,'rep'=4,'tp_0'=4,'tp_1'=2] {'fs_lo'}, dimensions={0}, use_global_device_ids=true | all-gather | bytes 81920 | tf_op jit(solution)/shard_map/left/all_gather | solution.py:312
  23.0 25.8 %all-gather.left = f32[16,16,256]{2,1,0:T(8,128)S(1)} all-gather(f32[4,16,256]{2,1,0:T(8,128)S(1)} %all_gather.16), channel_id=2, replica_groups=mesh['fs_hi'=4,'fs_lo'=4,'rep'=4,'tp_0'=4,'tp_1'=2] {'fs_hi'}, dimensions={0}, use_global_device_ids=true | all-gather | bytes 327680 | tf_op jit(solution)/shard_map/left/all_gather | solution.py:313
  48.9 0.0 copy-start
  48.9 0.0 copy-start.1
  48.9 0.0 copy-start.3
  48.9 0.0 copy-start.2
  48.9 0.0 copy-start.4
  48.9 0.0 all-to-all-done.arrived
  48.9 0.4 middle.1
  49.3 39.0 %all_to_all.20.arrived = f32[16,40,256]{2,1,0:T(8,128)S(1)} all-to-all(f32[16,40,256]{2,1,0:T(8,128)S(1)} %middle.1), channel_id=1, replica_groups=mesh['fs_hi'=4,'fs_lo'=4,'rep'=4,'tp_0'=4,'tp_1'=2] {'fs_hi','fs_lo'}, dimensions={0} | all-to-all | bytes 1310720 | tf_op jit(solution)/shard_map/far/all_to_all | solution.py:32
  88.3 0.0 copy-done
  88.3 0.0 copy-done.1
  88.3 0.0 copy-done.3
  88.3 1.1 settle.1
  89.4 9.6 %all-to-all-start.2 = ((f32[16,8,128]{2,1,0:T(8,128)}), f32[16,8,128]{2,1,0:T(8,128)S(1)}, u32[]{:S(2)}, u32[]{:S(2)}) async-start(f32[16,8,128]{2,1,0:T(8,128)} %get-tuple-element.18), calls=%async_computation.2 | async-start | bytes 131072 | tf_op jit(solution)/shard_map/sums/all_to_all | solution.py:32
  99.0 9.8 %all-gather.1 = f32[160,256]{1,0:T(8,128)S(1)} all-gather(f32[40,256]{1,0:T(8,128)S(1)} %get-tuple-element.19), channel_id=3, replica_groups=mesh['fs_hi'=4,'fs_lo'=4,'rep'=4,'tp_0'=4,'tp_1'=2] {'rep'}, dimensions={0}, use_global_device_ids=true | all-gather | bytes 204800 | tf_op jit(solution)/shard_map/share/all_gather | solution.py:328
  108.8 1.8 %all-to-all-done.2.tiles = f32[16,8,128]{2,1,0:T(8,128)S(1)} async-done(((f32[16,8,128]{2,1,0:T(8,128)}), f32[16,8,128]{2,1,0:T(8,128)S(1)}, u32[]{:S(2)}, u32[]{:S(2)}) %all-to-all-start.2) | async-done | bytes 65568 | tf_op jit(solution)/shard_map/sums/all_to_all | solution.py:32
  110.6 15.7 %all_to_all.21.sums = f32[32,8,128]{2,1,0:T(8,128)S(1)} all-to-all(f32[32,8,128]{2,1,0:T(8,128)S(1)} %sums.1), channel_id=1, replica_groups=mesh['fs_hi'=4,'fs_lo'=4,'rep'=4,'tp_0'=4,'tp_1'=2] {'rep','tp_0','tp_1'}, dimensions={0} | all-to-all | bytes 262144 | tf_op jit(solution)/shard_map/sums/all_to_all | solution.py:32
  126.4 0.0 copy-done.2
  126.4 0.0 copy-done.4
  126.4 1.1 update.1
  (2 shorter events, 0.0 us)
Async XLA Ops:
  6.6 5.1 %copy-start.5 = (bf16[1,16,256]{2,1,0:T(8,128)(2,1)S(1)}, bf16[1,16,256]{2,1,0:T(8,128)(2,1)}, u32[]{:S(2)}) copy-start(bf16[1,16,256]{2,1,0:T(8,128)(2,1)} %param.20) | copy-start | bytes 24580
  6.6 42.3 %all-to-all-start = ((f32[4,640,256]{2,1,0:T(8,128)}), f32[4,640,256]{2,1,0:T(8,128)S(1)}, u32[]{:S(2)}, u32[]{:S(2)}) async-start(f32[4,640,256]{2,1,0:T(8,128)} %product.1), calls=%async_computation | async-start | bytes 5242880 | tf_op jit(solution)/shard_map/near/all_to_all | solution.py:32
  48.9 39.4 %copy-start = (bf16[256,256]{1,0:T(8,128)(2,1)S(1)}, bf16[256,256]{1,0:T(8,128)(2,1)}, u32[]{:S(2)}) copy-start(bf16[256,256]{1,0:T(8,128)(2,1)} %rec_right.1) | copy-start | bytes 393220
  48.9 39.4 %copy-start.1 = (f32[128,256]{1,0:T(8,128)S(1)}, f32[128,256]{1,0:T(8,128)}, u32[]{:S(2)}) copy-start(f32[128,256]{1,0:T(8,128)} %rec_moment.1) | copy-start | bytes 393220
  48.9 39.4 %copy-start.3 = (f32[1,16,256]{2,1,0:T(8,128)S(1)}, f32[1,16,256]{2,1,0:T(8,128)}, u32[]{:S(2)}) copy-start(f32[1,16,256]{2,1,0:T(8,128)} %param.19) | copy-start | bytes 49156
  48.9 77.5 %copy-start.2 = (f32[128,256]{1,0:T(8,128)S(1)}, f32[128,256]{1,0:T(8,128)}, u32[]{:S(2)}) copy-start(f32[128,256]{1,0:T(8,128)} %rec_weight.1) | copy-start | bytes 393220
  48.9 77.5 %copy-start.4 = (f32[1,16,256]{2,1,0:T(8,128)S(1)}, f32[1,16,256]{2,1,0:T(8,128)}, u32[]{:S(2)}) copy-start(f32[1,16,256]{2,1,0:T(8,128)} %param.18) | copy-start | bytes 49156
  89.4 21.2 %all-to-all-start.2 = ((f32[16,8,128]{2,1,0:T(8,128)}), f32[16,8,128]{2,1,0:T(8,128)S(1)}, u32[]{:S(2)}, u32[]{:S(2)}) async-start(f32[16,8,128]{2,1,0:T(8,128)} %get-tuple-element.18), calls=%async_computation.2 | async-start | bytes 131072 | tf_op jit(solution)/shard_map/sums/all_to_all | solution.py:32

commit v4 on v3

--- a/solution.py
+++ b/solution.py
@@ -6,7 +6,6 @@
 from jax.sharding import Mesh
 from jax.sharding import PartitionSpec as P
 
-FS = ("fs_hi", "fs_lo")
 TP = ("tp_0", "tp_1")
 
 BETA = 0.9
@@ -52,62 +51,80 @@
     )(*args)
 
 
-def product_kernel(normed, rec_cot, conv_out, gate_cot, right, tiles, turned):
-    rep, rows, _ = tiles.shape
+def product_kernel(
+    normed, rec_cot, conv_hbm, cot_hbm, right_hbm, tiles, conv_out, gate_cot, right, sems
+):
+    rep, rows, block = tiles.shape
     group = pl.program_id(0)
+    copies = [
+        pltpu.make_async_copy(source, target, sems.at[i])
+        for i, (source, target) in enumerate(
+            ((conv_hbm, conv_out), (cot_hbm, gate_cot), (right_hbm, right))
+        )
+    ]
 
     @pl.when(group == 0)
     def _():
+        for copy in copies:
+            copy.start()
+
+    @pl.when(group < GROUPS)
+    def _():
+        part = lax.dot_general(
+            normed[...], rec_cot[...], ALONG_ROWS, preferred_element_type=F32
+        )
+        run = 128 // rep
+        for owner in range(rows // run):
+            for r in range(rep):
+                start = (owner * rep + r) * run
+                tiles[r, pl.ds(owner * run, run), :] = part[start : start + run]
+
+    @pl.when(group == GROUPS)
+    def _():
+        for copy in copies:
+            copy.wait()
         grad = lax.dot_general(
             gate_cot[...], conv_out[...], ALONG_ROWS, preferred_element_type=F32
         )
-        turned[0] = grad
-        turned[1] = lax.dot_general(
+        done = lax.dot_general(
             right[...].astype(F32),
             grad,
             ALONG_ROWS,
             precision=HIGH,
             preferred_element_type=F32,
         )
-
-    part = lax.dot_general(
-        normed[...], rec_cot[...], ALONG_ROWS, preferred_element_type=F32
-    )
-    share = turned.shape[1] // rep
-    piece = share // GROUPS
-    rec_rows = rows - 2 * piece
-    run = 128 // rep
-    for owner in range(rec_rows // run):
+        share = block // rep
         for r in range(rep):
-            start = (owner * rep + r) * run
-            tiles[r, pl.ds(owner * run, run), :] = part[start : start + run]
-    for r in range(rep):
-        at = pl.multiple_of(r * share + group * piece, piece)
-        for i in range(2):
-            tiles[r, pl.ds(rec_rows + i * piece, piece), :] = turned[
-                i, pl.ds(at, piece), :
-            ]
+            for i, value in enumerate((grad, done)):
+                tiles[r, pl.ds(i * share, share), :] = value[
+                    r * share : (r + 1) * share
+                ]
 
 
 def product(normed, rec_cot, conv_out, gate_cot, right, rep):
     tokens, width = normed.shape
     block = rec_cot.shape[1]
-    rows = (width + 2 * block) // rep
-    fixed = pl.BlockSpec((tokens, block), lambda g: (0, 0))
+    rows = width // GROUPS // rep
     flops = 2 * tokens * block * (width + block)
+    held = lambda value: pltpu.VMEM(value.shape, value.dtype)
     return pl.pallas_call(
         product_kernel,
-        grid=(GROUPS,),
+        grid=(GROUPS + 1,),
         in_specs=[
-            pl.BlockSpec((tokens, width // GROUPS), lambda g: (0, g)),
-            fixed,
-            fixed,
-            fixed,
-            pl.BlockSpec((block, block), lambda g: (0, 0)),
+            pl.BlockSpec(
+                (tokens, width // GROUPS), lambda g: (0, jnp.minimum(g, GROUPS - 1))
+            ),
+            pl.BlockSpec((tokens, block), lambda g: (0, 0)),
+            *[pl.BlockSpec(memory_space=pl.ANY)] * 3,
         ],
-        out_specs=pl.BlockSpec((rep, rows // GROUPS, block), lambda g: (0, g, 0)),
-        out_shape=jax.ShapeDtypeStruct((rep, rows, block), F32),
-        scratch_shapes=[pltpu.VMEM((2, block, block), F32)],
+        out_specs=pl.BlockSpec((rep, rows, block), lambda g: (0, g, 0)),
+        out_shape=jax.ShapeDtypeStruct((rep, rows * (GROUPS + 1), block), F32),
+        scratch_shapes=[
+            held(conv_out),
+            held(gate_cot),
+            held(right),
+            pltpu.SemaphoreType.DMA((3,)),
+        ],
         cost_estimate=pl.CostEstimate(
             flops=flops, bytes_accessed=1 << 22, transcendentals=0
         ),
@@ -117,26 +134,20 @@
 def middle_kernel(arrived, left, tiles):
     rep = arrived.shape[0]
     fs, _, block = tiles.shape
-    rows = arrived.shape[1] // GROUPS
-    share = block // rep
-    piece = share // GROUPS
-    rec_rows = rows - 2 * piece
-    owners = fs // GROUPS
-    run = rec_rows // owners
-    half = block // 2
-    grads, rights = [], []
-    for g in range(GROUPS):
-        total = arrived[0, pl.ds(g * rows, rows), :]
+    half, share = block // 2, block // rep
+    rec_rows = arrived.shape[1] - 2 * share
+    run = rec_rows // fs
+
+    def total(start, size):
+        value = arrived[0, pl.ds(start, size), :]
         for r in range(1, rep):
-            total += arrived[r, pl.ds(g * rows, rows), :]
-        for owner in range(owners):
-            tiles[g * owners + owner, pl.ds(0, run), :] = total[
-                owner * run : (owner + 1) * run
-            ]
-        grads.append(total[rec_rows : rec_rows + piece])
-        rights.append(total[rec_rows + piece :])
-    turned = jnp.concatenate(grads, axis=0)
-    right_done = jnp.concatenate(rights, axis=0)
+            value += arrived[r, pl.ds(start, size), :]
+        return value
+
+    for f in range(fs):
+        tiles[f, pl.ds(0, run), :] = total(f * run, run)
+    turned = total(rec_rows, share)
+    right_done = total(rec_rows + share, share)
     blank = jnp.zeros_like(right_done)
     depth = left.shape[1] // 2
     done = None
@@ -299,35 +310,33 @@
     gate_left,
     gate_right,
 ):
-    fs, rep = size_of(FS), lax.axis_size("rep")
+    fs, rep = lax.axis_size("fs"), lax.axis_size("rep")
     like = lambda value, kind=F32: jax.ShapeDtypeStruct(value.shape, kind)
     gate_weight, gate_moment = gate_weight[0], gate_moment[0]
-    own_rows, block = gate_weight.shape
 
     with jax.named_scope("product"):
         tiles = product(normed, rec_cot, conv_out, gate_cot, gate_right[0], rep)
     with jax.named_scope("near"):
         arrived = exchange(tiles, "rep")
     with jax.named_scope("left"):
-        left = lax.all_gather(gate_left[0].astype(F32), "fs_lo")
-        left = lax.all_gather(left, "fs_hi").reshape(fs, own_rows, block)
+        left = lax.all_gather(gate_left[0].astype(F32), "fs", tiled=True).reshape(fs, *gate_left.shape[1:])
     with jax.named_scope("middle"):
         tiles = middle(arrived, left)
     with jax.named_scope("far"):
-        arrived = exchange(tiles, FS)
+        arrived = exchange(tiles, "fs")
     with jax.named_scope("settle"):
         mine, sums = on_core(
             settle_kernel,
             (
                 jax.ShapeDtypeStruct(arrived.shape[1:], F32),
-                jax.ShapeDtypeStruct((fs, 8, 128), F32),
+                jax.ShapeDtypeStruct((fs, 4, 128), F32),
             ),
             (arrived, rec_right, rec_moment, gate_moment),
         )
     with jax.named_scope("share"):
         full = lax.all_gather(mine, "rep")
     with jax.named_scope("sums"):
-        sums = fold(exchange(sums, FS), rep * size_of(TP), full)
+        sums = fold(exchange(sums, "fs"), rep * size_of(TP), full)
         sums = exchange(sums, ("rep", *TP))
     with jax.named_scope("update"):
         bf16 = jnp.bfloat16
@@ -369,21 +378,21 @@
 def solution(mesh):
     fs, rep, tp = (mesh.shape[name] for name in ("fs", "rep", "tp"))
     split = Mesh(
-        mesh.devices.reshape(fs // 4, 4, rep, tp // 2, 2),
-        (*FS, "rep", *TP),
-    )
-    tokens = (*FS, "rep")
+        mesh.devices.reshape(fs, rep, tp // 2, 2),
+        ("fs", "rep", *TP),
+    )
+    tokens = ("fs", "rep")
     placed = (
         P(tokens, None),
         P(tokens, TP),
         P(tokens, TP),
         P(tokens, TP),
-        P(FS, TP),
-        P(FS, TP),
+        P("fs", TP),
+        P("fs", TP),
         P(TP, None),
-        P(TP, FS, None),
-        P(TP, FS, None),
-        P(TP, FS, None),
+        P(TP, "fs", None),
+        P(TP, "fs", None),
+        P(TP, "fs", None),
         P(TP, None, None),
     )
 
@@ -391,6 +400,6 @@
         shards,
         mesh=split,
         in_specs=placed,
-        out_specs=(P(FS, TP),) * 4 + (P(TP, FS, None),) * 4,
+        out_specs=(P("fs", TP),) * 4 + (P(TP, "fs", None),) * 4,
         check_vma=False,
     )

time: 128 us -> 127 us (level)
  starting transfers between devices: 14.8 us -> 11.9 us
  blocking collectives: 102 us -> 104 us
    all_to_all x2, blocking collectives: 54.7 us -> 62.4 us  [exchange(): return lax.all_to_all(tiles, axes, split_axis=0, concat_axis=0, tiled=True)]
    all_gather x2 -> x1, blocking collectives: 37.2 us -> 31.7 us  [shards(): lax.all_gather(gate_left[0].astype(F32), 'fs', tiled=True)]
    all_to_all x2, starting transfers between devices: 14.8 us -> 11.9 us  [exchange(): return lax.all_to_all(tiles, axes, split_axis=0, concat_axis=0, tiled=True)]
where the time goes in v4:
time: 127 us
  blocking collectives  104 us (82%)
  starting transfers between devices  11.9 us (9%)
  Pallas kernels  8.44 us (7%)
  waiting for transfers between devices  1.71 us (1%)
    all_to_all x2, blocking collectives, exchange(): return lax.all_to_all(tiles, axes, split_axis=0, concat_axis=0, tiled=True)  62.4 us
    all_gather x1, blocking collectives, shards(): lax.all_gather(gate_left[0].astype(F32), 'fs', tiled=True)  31.7 us
    all_to_all x2, starting transfers between devices, exchange(): return lax.all_to_all(tiles, axes, split_axis=0, concat_axis=0, tiled=True)  11.9 us
    all_gather x1, blocking collectives, shards(): full = lax.all_gather(mine, 'rep')  9.76 us
    pallas_call x1, Pallas kernels, product(): pl.pallas_call(product_kernel, grid=(GROUPS + 1,), in_specs=[pl.BlockSpec...  5.85 us
    pallas_call x4, Pallas kernels, on_core(): pl.pallas_call(kernel, out_shape=outs[0] if single else outs, in_specs=[w...  2.59 us
  transfers between devices with their start and end apart: 2, of which 1 were waited for; matrix products, arithmetic and copies ran while one was open for 0% of the time, Pallas kernels for 0%

profile of v4, /device:TPU:1, one launch (start us, length us, event | category | flops | bytes accessed | tf_op | source)
XLA Modules:
  0.0 126.7 jit_solution(1090883914618599345)
XLA Ops:
  0.6 5.9 %product.1 = f32[4,640,256]{2,1,0:T(8,128)} custom-call(bf16[640,2048]{1,0:T(8,128)(2,1)} %normed.1, bf16[640,256]{1,0:T(8,128)(2,1)} %rec_cot.1, bf16[640,256]{1,0:T(8,128)(2,1)} %conv_hbm.1, bf16[640,256]{1,0:T(8,128)(2,1)} %cot_hbm.1, bf16[256,256]{1,0:T(8,128)(2,1)} %bitcast.14), custom_call_target="tpu_custom_call" | custom-call | flops 754974720 | bytes 4194304 | tf_op jit(solution)/shard_map/product/pallas_call | solution.py:110
  6.5 0.0 copy-start.5
  6.5 5.0 %all-to-all-start = ((f32[4,640,256]{2,1,0:T(8,128)}), f32[4,640,256]{2,1,0:T(8,128)S(1)}, u32[]{:S(2)}, u32[]{:S(2)}) async-start(f32[4,640,256]{2,1,0:T(8,128)} %product.1), calls=%async_computation | async-start | bytes 5242880 | tf_op jit(solution)/shard_map/near/all_to_all | solution.py:31
  11.5 0.0 copy-done.5
  11.5 31.7 %all-gather = f32[1,256,256]{2,1,0:T(8,128)S(1)} all-gather(f32[1,16,256]{2,1,0:T(8,128)S(1)} %convert_element_type.8), channel_id=2, replica_groups=mesh['fs'=16,'rep'=4,'tp_0'=4,'tp_1'=2] {'fs'}, dimensions={1}, use_global_device_ids=true | all-gather | bytes 278528 | tf_op jit(solution)/shard_map/left/all_gather | solution.py:322
  43.3 0.0 all-to-all-done.arrived
  43.3 0.0 copy-start
  43.3 0.0 copy-start.1
  43.3 0.0 copy-start.3
  43.3 0.0 copy-start.2
  43.3 0.0 copy-start.4
  43.3 0.4 middle.1
  43.7 47.9 %all_to_all.20.arrived = f32[16,40,256]{2,1,0:T(8,128)S(1)} all-to-all(f32[16,40,256]{2,1,0:T(8,128)S(1)} %middle.1), channel_id=1, replica_groups=mesh['fs'=16,'rep'=4,'tp_0'=4,'tp_1'=2] {'fs'}, dimensions={0} | all-to-all | bytes 1310720 | tf_op jit(solution)/shard_map/far/all_to_all | solution.py:31
  91.5 0.0 copy-done
  91.5 0.0 copy-done.1
  91.5 0.0 copy-done.3
  91.6 1.1 settle.1
  92.7 6.9 %all-to-all-start.2 = ((f32[16,4,128]{2,1,0:T(4,128)}), f32[16,4,128]{2,1,0:T(4,128)S(1)}, u32[]{:S(2)}, u32[]{:S(2)}) async-start(f32[16,4,128]{2,1,0:T(4,128)} %get-tuple-element.18), calls=%async_computation.2 | async-start | bytes 65536 | tf_op jit(solution)/shard_map/sums/all_to_all | solution.py:31
  99.6 9.8 %all-gather.1 = f32[160,256]{1,0:T(8,128)S(1)} all-gather(f32[40,256]{1,0:T(8,128)S(1)} %get-tuple-element.19), channel_id=3, replica_groups=mesh['fs'=16,'rep'=4,'tp_0'=4,'tp_1'=2] {'rep'}, dimensions={0}, use_global_device_ids=true | all-gather | bytes 204800 | tf_op jit(solution)/shard_map/share/all_gather | solution.py:337
  109.3 1.7 %all-to-all-done.2.tiles = f32[16,4,128]{2,1,0:T(4,128)S(1)} async-done(((f32[16,4,128]{2,1,0:T(4,128)}), f32[16,4,128]{2,1,0:T(4,128)S(1)}, u32[]{:S(2)}, u32[]{:S(2)}) %all-to-all-start.2) | async-done | bytes 32800 | tf_op jit(solution)/shard_map/sums/all_to_all | solution.py:31
  111.1 14.6 %all_to_all.21.sums = f32[32,4,128]{2,1,0:T(4,128)S(1)} all-to-all(f32[32,4,128]{2,1,0:T(4,128)S(1)} %sums.1), channel_id=1, replica_groups=mesh['fs'=16,'rep'=4,'tp_0'=4,'tp_1'=2] {'rep','tp_0','tp_1'}, dimensions={0} | all-to-all | bytes 131072 | tf_op jit(solution)/shard_map/sums/all_to_all | solution.py:31
  125.6 0.0 copy-done.2
  125.6 0.0 copy-done.4
  125.6 1.1 update.1
  (2 shorter events, 0.0 us)
Async XLA Ops:
  6.5 5.0 %copy-start.5 = (bf16[1,16,256]{2,1,0:T(8,128)(2,1)S(1)}, bf16[1,16,256]{2,1,0:T(8,128)(2,1)}, u32[]{:S(2)}) copy-start(bf16[1,16,256]{2,1,0:T(8,128)(2,1)} %param.20) | copy-start | bytes 24580
  6.5 36.8 %all-to-all-start = ((f32[4,640,256]{2,1,0:T(8,128)}), f32[4,640,256]{2,1,0:T(8,128)S(1)}, u32[]{:S(2)}, u32[]{:S(2)}) async-start(f32[4,640,256]{2,1,0:T(8,128)} %product.1), calls=%async_computation | async-start | bytes 5242880 | tf_op jit(solution)/shard_map/near/all_to_all | solution.py:31
  43.3 48.3 %copy-start = (bf16[256,256]{1,0:T(8,128)(2,1)S(1)}, bf16[256,256]{1,0:T(8,128)(2,1)}, u32[]{:S(2)}) copy-start(bf16[256,256]{1,0:T(8,128)(2,1)} %rec_right.1) | copy-start | bytes 393220
  43.3 48.3 %copy-start.1 = (f32[128,256]{1,0:T(8,128)S(1)}, f32[128,256]{1,0:T(8,128)}, u32[]{:S(2)}) copy-start(f32[128,256]{1,0:T(8,128)} %rec_moment.1) | copy-start | bytes 393220
  43.3 48.3 %copy-start.3 = (f32[1,16,256]{2,1,0:T(8,128)S(1)}, f32[1,16,256]{2,1,0:T(8,128)}, u32[]{:S(2)}) copy-start(f32[1,16,256]{2,1,0:T(8,128)} %param.19) | copy-start | bytes 49156
  43.3 82.4 %copy-start.2 = (f32[128,256]{1,0:T(8,128)S(1)}, f32[128,256]{1,0:T(8,128)}, u32[]{:S(2)}) copy-start(f32[128,256]{1,0:T(8,128)} %rec_weight.1) | copy-start | bytes 393220
  43.3 82.4 %copy-start.4 = (f32[1,16,256]{2,1,0:T(8,128)S(1)}, f32[1,16,256]{2,1,0:T(8,128)}, u32[]{:S(2)}) copy-start(f32[1,16,256]{2,1,0:T(8,128)} %param.18) | copy-start | bytes 49156
  92.7 18.4 %all-to-all-start.2 = ((f32[16,4,128]{2,1,0:T(4,128)}), f32[16,4,128]{2,1,0:T(4,128)S(1)}, u32[]{:S(2)}, u32[]{:S(2)}) async-start(f32[16,4,128]{2,1,0:T(4,128)} %get-tuple-element.18), calls=%async_computation.2 | async-start | bytes 65536 | tf_op jit(solution)/shard_map/sums/all_to_all | solution.py:31

commit v5 on v4

--- a/solution.py
+++ b/solution.py
@@ -6,6 +6,7 @@
 from jax.sharding import Mesh
 from jax.sharding import PartitionSpec as P
 
+FS = ("fs_hi", "fs_lo")
 TP = ("tp_0", "tp_1")
 
 BETA = 0.9
@@ -144,8 +145,10 @@
             value += arrived[r, pl.ds(start, size), :]
         return value
 
+    lo = lax.axis_size("fs_lo")
+    place = [f % lo * (fs // lo) + f // lo for f in range(fs)]
     for f in range(fs):
-        tiles[f, pl.ds(0, run), :] = total(f * run, run)
+        tiles[place[f], pl.ds(0, run), :] = total(f * run, run)
     turned = total(rec_rows, share)
     right_done = total(rec_rows + share, share)
     blank = jnp.zeros_like(right_done)
@@ -164,10 +167,10 @@
         done = term if done is None else done + term
     for f in range(fs):
         row, side = f // 2 * depth, f % 2 * half
-        tiles[f, pl.ds(run, depth), pl.ds(0, half)] = turned[
+        tiles[place[f], pl.ds(run, depth), pl.ds(0, half)] = turned[
             row : row + depth, side : side + half
         ]
-        tiles[f, pl.ds(run, depth), pl.ds(half, half)] = done[
+        tiles[place[f], pl.ds(run, depth), pl.ds(half, half)] = done[
             f * depth : (f + 1) * depth
         ]
 
@@ -177,6 +180,19 @@
     rec_rows = arrived.shape[1] - 2 * block // arrived.shape[0]
     out = jax.ShapeDtypeStruct((fs, rec_rows // fs + own_rows // 2, block), F32)
     return on_core(middle_kernel, (out,), (arrived, left), flops=1 << 30)
+
+
+def add_kernel(tiles, total):
+    value = tiles[0]
+    for i in range(1, tiles.shape[0]):
+        value += tiles[i]
+    total[...] = value
+
+
+def add_up(tiles):
+    return on_core(
+        add_kernel, (jax.ShapeDtypeStruct(tiles.shape[1:], F32),), (tiles,)
+    )
 
 
 def fold_kernel(tiles, after, copies):
@@ -310,7 +326,7 @@
     gate_left,
     gate_right,
 ):
-    fs, rep = lax.axis_size("fs"), lax.axis_size("rep")
+    fs, rep = size_of(FS), lax.axis_size("rep")
     like = lambda value, kind=F32: jax.ShapeDtypeStruct(value.shape, kind)
     gate_weight, gate_moment = gate_weight[0], gate_moment[0]
 
@@ -319,11 +335,15 @@
     with jax.named_scope("near"):
         arrived = exchange(tiles, "rep")
     with jax.named_scope("left"):
-        left = lax.all_gather(gate_left[0].astype(F32), "fs", tiled=True).reshape(fs, *gate_left.shape[1:])
+        left = lax.all_gather(gate_left[0].astype(F32), FS, tiled=True).reshape(fs, *gate_left.shape[1:])
     with jax.named_scope("middle"):
         tiles = middle(arrived, left)
+    with jax.named_scope("quarter"):
+        hi, lo = lax.axis_size("fs_hi"), lax.axis_size("fs_lo")
+        rows = tiles.shape[1]
+        tiles = add_up(exchange(tiles.reshape(lo, hi * rows, -1), "fs_lo"))
     with jax.named_scope("far"):
-        arrived = exchange(tiles, "fs")
+        arrived = exchange(tiles.reshape(hi, rows, -1), "fs_hi")
     with jax.named_scope("settle"):
         mine, sums = on_core(
             settle_kernel,
@@ -336,7 +356,7 @@
     with jax.named_scope("share"):
         full = lax.all_gather(mine, "rep")
     with jax.named_scope("sums"):
-        sums = fold(exchange(sums, "fs"), rep * size_of(TP), full)
+        sums = fold(exchange(sums, FS), rep * size_of(TP), full)
         sums = exchange(sums, ("rep", *TP))
     with jax.named_scope("update"):
         bf16 = jnp.bfloat16
@@ -378,21 +398,21 @@
 def solution(mesh):
     fs, rep, tp = (mesh.shape[name] for name in ("fs", "rep", "tp"))
     split = Mesh(
-        mesh.devices.reshape(fs, rep, tp // 2, 2),
-        ("fs", "rep", *TP),
-    )
-    tokens = ("fs", "rep")
+        mesh.devices.reshape(fs // 4, 4, rep, tp // 2, 2),
+        (*FS, "rep", *TP),
+    )
+    tokens = (*FS, "rep")
     placed = (
         P(tokens, None),
         P(tokens, TP),
         P(tokens, TP),
         P(tokens, TP),
-        P("fs", TP),
-        P("fs", TP),
+        P(FS, TP),
+        P(FS, TP),
         P(TP, None),
-        P(TP, "fs", None),
-        P(TP, "fs", None),
-        P(TP, "fs", None),
+        P(TP, FS, None),
+        P(TP, FS, None),
+        P(TP, FS, None),
         P(TP, None, None),
     )
 
@@ -400,6 +420,6 @@
         shards,
         mesh=split,
         in_specs=placed,
-        out_specs=(P("fs", TP),) * 4 + (P(TP, "fs", None),) * 4,
+        out_specs=(P(FS, TP),) * 4 + (P(TP, FS, None),) * 4,
         check_vma=False,
     )

time: 127 us -> 126 us (level)
  starting transfers between devices: 11.9 us -> 9 us
    all_to_all x2, starting transfers between devices: 11.9 us -> 9 us  [exchange(): return lax.all_to_all(tiles, axes, split_axis=0, concat_axis=0, tiled=True)]
    all_to_all x2 -> x3, blocking collectives: 62.4 us -> 64.3 us  [exchange(): return lax.all_to_all(tiles, axes, split_axis=0, concat_axis=0, tiled=True)]
    pallas_call x4 -> x5, Pallas kernels: 2.59 us -> 2.6 us  [on_core(): pl.pallas_call(kernel, out_shape=outs[0] if single else outs, in_specs=[w...]
where the time goes in v5:
time: 126 us
  blocking collectives  105 us (83%)
  starting transfers between devices  9 us (7%)
  Pallas kernels  8.45 us (7%)
  waiting for transfers between devices  2.01 us (2%)
    all_to_all x3, blocking collectives, exchange(): return lax.all_to_all(tiles, axes, split_axis=0, concat_axis=0, tiled=True)  64.3 us
    all_gather x1, blocking collectives, shards(): lax.all_gather(gate_left[0].astype(F32), FS, tiled=True)  31.7 us
    all_gather x1, blocking collectives, shards(): full = lax.all_gather(mine, 'rep')  9.47 us
    all_to_all x2, starting transfers between devices, exchange(): return lax.all_to_all(tiles, axes, split_axis=0, concat_axis=0, tiled=True)  9 us
    pallas_call x1, Pallas kernels, product(): pl.pallas_call(product_kernel, grid=(GROUPS + 1,), in_specs=[pl.BlockSpec...  5.85 us
    pallas_call x5, Pallas kernels, on_core(): pl.pallas_call(kernel, out_shape=outs[0] if single else outs, in_specs=[w...  2.6 us
  transfers between devices with their start and end apart: 2, of which 1 were waited for; matrix products, arithmetic and copies ran while one was open for 0% of the time, Pallas kernels for 0%

profile of v5, /device:TPU:1, one launch (start us, length us, event | category | flops | bytes accessed | tf_op | source)
XLA Modules:
  0.0 125.7 jit_solution(1454430497562845712)
XLA Ops:
  0.6 5.9 %product.1 = f32[4,640,256]{2,1,0:T(8,128)} custom-call(bf16[640,2048]{1,0:T(8,128)(2,1)} %normed.1, bf16[640,256]{1,0:T(8,128)(2,1)} %rec_cot.1, bf16[640,256]{1,0:T(8,128)(2,1)} %conv_hbm.1, bf16[640,256]{1,0:T(8,128)(2,1)} %cot_hbm.1, bf16[256,256]{1,0:T(8,128)(2,1)} %bitcast.18), custom_call_target="tpu_custom_call" | custom-call | flops 754974720 | bytes 4194304 | tf_op jit(solution)/shard_map/product/pallas_call | solution.py:111
  6.5 0.0 copy-start.5
  6.5 5.0 %all-to-all-start = ((f32[4,640,256]{2,1,0:T(8,128)}), f32[4,640,256]{2,1,0:T(8,128)S(1)}, u32[]{:S(2)}, u32[]{:S(2)}) async-start(f32[4,640,256]{2,1,0:T(8,128)} %product.1), calls=%async_computation | async-start | bytes 5242880 | tf_op jit(solution)/shard_map/near/all_to_all | solution.py:32
  11.5 0.0 copy-done.5
  11.5 31.7 %all-gather = f32[1,256,256]{2,1,0:T(8,128)S(1)} all-gather(f32[1,16,256]{2,1,0:T(8,128)S(1)} %convert_element_type.8), channel_id=2, replica_groups=mesh['fs_hi'=4,'fs_lo'=4,'rep'=4,'tp_0'=4,'tp_1'=2] {'fs_hi','fs_lo'}, dimensions={1}, use_global_device_ids=true | all-gather | bytes 278528 | tf_op jit(solution)/shard_map/left/all_gather | solution.py:338
  43.3 0.0 all-to-all-done.arrived
  43.3 0.0 copy-start
  43.3 0.0 copy-start.1
  43.3 0.0 copy-start.3
  43.3 0.4 middle.1
  43.6 0.0 copy-start.2
  43.7 0.0 copy-start.4
  43.7 20.5 %all_to_all.25.tiles = f32[4,160,256]{2,1,0:T(8,128)S(1)} all-to-all(f32[4,160,256]{2,1,0:T(8,128)S(1)} %bitcast.13), channel_id=1, replica_groups=mesh['fs_hi'=4,'fs_lo'=4,'rep'=4,'tp_0'=4,'tp_1'=2] {'fs_lo'}, dimensions={0} | all-to-all | bytes 1310720 | tf_op jit(solution)/shard_map/quarter/all_to_all | solution.py:32
  64.2 26.6 %all_to_all.26.arrived = f32[4,40,256]{2,1,0:T(8,128)S(1)} all-to-all(f32[4,40,256]{2,1,0:T(8,128)S(1)} %bitcast.14), channel_id=1, replica_groups=mesh['fs_hi'=4,'fs_lo'=4,'rep'=4,'tp_0'=4,'tp_1'=2] {'fs_hi'}, dimensions={0} | all-to-all | bytes 327680 | tf_op jit(solution)/shard_map/far/all_to_all | solution.py:32
  90.8 0.0 copy-done
  90.8 0.0 copy-done.1
  90.8 0.0 copy-done.3
  90.8 1.1 settle.1
  91.9 4.0 %all-to-all-start.3 = ((f32[16,4,128]{2,1,0:T(4,128)}), f32[16,4,128]{2,1,0:T(4,128)S(1)}, u32[]{:S(2)}, u32[]{:S(2)}) async-start(f32[16,4,128]{2,1,0:T(4,128)} %get-tuple-element.18), calls=%async_computation.3 | async-start | bytes 65536 | tf_op jit(solution)/shard_map/sums/all_to_all | solution.py:32
  95.9 9.5 %all-gather.1 = f32[160,256]{1,0:T(8,128)S(1)} all-gather(f32[40,256]{1,0:T(8,128)S(1)} %get-tuple-element.19), channel_id=3, replica_groups=mesh['fs_hi'=4,'fs_lo'=4,'rep'=4,'tp_0'=4,'tp_1'=2] {'rep'}, dimensions={0}, use_global_device_ids=true | all-gather | bytes 204800 | tf_op jit(solution)/shard_map/share/all_gather | solution.py:357
  105.4 2.0 %all-to-all-done.3.tiles = f32[16,4,128]{2,1,0:T(4,128)S(1)} async-done(((f32[16,4,128]{2,1,0:T(4,128)}), f32[16,4,128]{2,1,0:T(4,128)S(1)}, u32[]{:S(2)}, u32[]{:S(2)}) %all-to-all-start.3) | async-done | bytes 32800 | tf_op jit(solution)/shard_map/sums/all_to_all | solution.py:32
  107.4 17.2 %all_to_all.27.sums = f32[32,4,128]{2,1,0:T(4,128)S(1)} all-to-all(f32[32,4,128]{2,1,0:T(4,128)S(1)} %sums.1), channel_id=1, replica_groups=mesh['fs_hi'=4,'fs_lo'=4,'rep'=4,'tp_0'=4,'tp_1'=2] {'rep','tp_0','tp_1'}, dimensions={0} | all-to-all | bytes 131072 | tf_op jit(solution)/shard_map/sums/all_to_all | solution.py:32
  124.6 0.0 copy-done.2
  124.6 0.0 copy-done.4
  124.6 1.1 update.1
  (3 shorter events, 0.1 us)
Async XLA Ops:
  6.5 5.0 %copy-start.5 = (bf16[1,16,256]{2,1,0:T(8,128)(2,1)S(1)}, bf16[1,16,256]{2,1,0:T(8,128)(2,1)}, u32[]{:S(2)}) copy-start(bf16[1,16,256]{2,1,0:T(8,128)(2,1)} %param.20) | copy-start | bytes 24580
  6.5 36.8 %all-to-all-start = ((f32[4,640,256]{2,1,0:T(8,128)}), f32[4,640,256]{2,1,0:T(8,128)S(1)}, u32[]{:S(2)}, u32[]{:S(2)}) async-start(f32[4,640,256]{2,1,0:T(8,128)} %product.1), calls=%async_computation | async-start | bytes 5242880 | tf_op jit(solution)/shard_map/near/all_to_all | solution.py:32
  43.3 47.5 %copy-start = (bf16[256,256]{1,0:T(8,128)(2,1)S(1)}, bf16[256,256]{1,0:T(8,128)(2,1)}, u32[]{:S(2)}) copy-start(bf16[256,256]{1,0:T(8,128)(2,1)} %rec_right.1) | copy-start | bytes 393220
  43.3 47.5 %copy-start.1 = (f32[128,256]{1,0:T(8,128)S(1)}, f32[128,256]{1,0:T(8,128)}, u32[]{:S(2)}) copy-start(f32[128,256]{1,0:T(8,128)} %rec_moment.1) | copy-start | bytes 393220
  43.3 47.5 %copy-start.3 = (f32[1,16,256]{2,1,0:T(8,128)S(1)}, f32[1,16,256]{2,1,0:T(8,128)}, u32[]{:S(2)}) copy-start(f32[1,16,256]{2,1,0:T(8,128)} %param.19) | copy-start | bytes 49156
  43.6 81.0 %copy-start.2 = (f32[128,256]{1,0:T(8,128)S(1)}, f32[128,256]{1,0:T(8,128)}, u32[]{:S(2)}) copy-start(f32[128,256]{1,0:T(8,128)} %rec_weight.1) | copy-start | bytes 393220
  43.7 81.0 %copy-start.4 = (f32[1,16,256]{2,1,0:T(8,128)S(1)}, f32[1,16,256]{2,1,0:T(8,128)}, u32[]{:S(2)}) copy-start(f32[1,16,256]{2,1,0:T(8,128)} %param.18) | copy-start | bytes 49156
  91.9 15.5 %all-to-all-start.3 = ((f32[16,4,128]{2,1,0:T(4,128)}), f32[16,4,128]{2,1,0:T(4,128)S(1)}, u32[]{:S(2)}, u32[]{:S(2)}) async-start(f32[16,4,128]{2,1,0:T(4,128)} %get-tuple-element.18), calls=%async_computation.3 | async-start | bytes 65536 | tf_op jit(solution)/shard_map/sums/all_to_all | solution.py:32

commit v6 on v5

--- a/solution.py
+++ b/solution.py
@@ -12,7 +12,7 @@
 BETA = 0.9
 LEARN_RATE = 0.02
 EPSILON = 1e-06
-GROUPS = 4
+PIECES = 4
 GRANT = 16 << 20
 F32 = jnp.float32
 HIGH = lax.Precision.HIGHEST
@@ -53,83 +53,103 @@
 
 
 def product_kernel(
-    normed, rec_cot, conv_hbm, cot_hbm, right_hbm, tiles, conv_out, gate_cot, right, sems
+    normed_hbm,
+    cot_hbm,
+    conv_hbm,
+    gate_hbm,
+    right_hbm,
+    tiles_hbm,
+    normed,
+    rec_cot,
+    conv_out,
+    gate_cot,
+    right,
+    tiles,
+    in_sems,
+    out_sems,
 ):
     rep, rows, block = tiles.shape
-    group = pl.program_id(0)
-    copies = [
-        pltpu.make_async_copy(source, target, sems.at[i])
+    share = block // rep
+    rec_rows = rows - 2 * share
+    step = rec_rows // PIECES
+    run = 128 // rep
+
+    small = [
+        pltpu.make_async_copy(source, target, in_sems.at[i])
         for i, (source, target) in enumerate(
-            ((conv_hbm, conv_out), (cot_hbm, gate_cot), (right_hbm, right))
+            (
+                (conv_hbm, conv_out),
+                (gate_hbm, gate_cot),
+                (right_hbm, right),
+                (cot_hbm, rec_cot),
+            )
         )
     ]
-
-    @pl.when(group == 0)
-    def _():
-        for copy in copies:
-            copy.start()
-
-    @pl.when(group < GROUPS)
-    def _():
-        part = lax.dot_general(
-            normed[...], rec_cot[...], ALONG_ROWS, preferred_element_type=F32
-        )
-        run = 128 // rep
-        for owner in range(rows // run):
+    large = pltpu.make_async_copy(normed_hbm, normed, in_sems.at[len(small)])
+    for copy in (*small, large):
+        copy.start()
+
+    def send(start, size, i):
+        part = (slice(None), pl.ds(start, size), slice(None))
+        copy = pltpu.make_async_copy(tiles.at[part], tiles_hbm.at[part], out_sems.at[i])
+        copy.start()
+        return copy
+
+    sent = []
+    for copy in small:
+        copy.wait()
+    grad = lax.dot_general(
+        gate_cot[...], conv_out[...], ALONG_ROWS, preferred_element_type=F32
+    )
+    done = lax.dot_general(
+        right[...].astype(F32),
+        grad,
+        ALONG_ROWS,
+        precision=HIGH,
+        preferred_element_type=F32,
+    )
+    for r in range(rep):
+        for i, value in enumerate((grad, done)):
+            tiles[r, pl.ds(rec_rows + i * share, share), :] = value[
+                r * share : (r + 1) * share
+            ]
+    sent.append(send(rec_rows, 2 * share, PIECES))
+    large.wait()
+    part = lax.dot_general(
+        normed[...], rec_cot[...], ALONG_ROWS, preferred_element_type=F32
+    )
+    for piece in range(PIECES):
+        for owner in range(piece * step // run, (piece + 1) * step // run):
             for r in range(rep):
                 start = (owner * rep + r) * run
                 tiles[r, pl.ds(owner * run, run), :] = part[start : start + run]
-
-    @pl.when(group == GROUPS)
-    def _():
-        for copy in copies:
-            copy.wait()
-        grad = lax.dot_general(
-            gate_cot[...], conv_out[...], ALONG_ROWS, preferred_element_type=F32
-        )
-        done = lax.dot_general(
-            right[...].astype(F32),
-            grad,
-            ALONG_ROWS,
-            precision=HIGH,
-            preferred_element_type=F32,
-        )
-        share = block // rep
-        for r in range(rep):
-            for i, value in enumerate((grad, done)):
-                tiles[r, pl.ds(i * share, share), :] = value[
-                    r * share : (r + 1) * share
-                ]
+        sent.append(send(piece * step, step, piece))
+    for copy in sent:
+        copy.wait()
 
 
 def product(normed, rec_cot, conv_out, gate_cot, right, rep):
     tokens, width = normed.shape
     block = rec_cot.shape[1]
-    rows = width // GROUPS // rep
-    flops = 2 * tokens * block * (width + block)
-    held = lambda value: pltpu.VMEM(value.shape, value.dtype)
+    rows = (width + 2 * block) // rep
+    args = (normed, rec_cot, conv_out, gate_cot, right)
     return pl.pallas_call(
         product_kernel,
-        grid=(GROUPS + 1,),
-        in_specs=[
-            pl.BlockSpec(
-                (tokens, width // GROUPS), lambda g: (0, jnp.minimum(g, GROUPS - 1))
-            ),
-            pl.BlockSpec((tokens, block), lambda g: (0, 0)),
-            *[pl.BlockSpec(memory_space=pl.ANY)] * 3,
-        ],
-        out_specs=pl.BlockSpec((rep, rows, block), lambda g: (0, g, 0)),
-        out_shape=jax.ShapeDtypeStruct((rep, rows * (GROUPS + 1), block), F32),
+        in_specs=[pl.BlockSpec(memory_space=pl.ANY)] * len(args),
+        out_specs=pl.BlockSpec(memory_space=pl.ANY),
+        out_shape=jax.ShapeDtypeStruct((rep, rows, block), F32),
         scratch_shapes=[
-            held(conv_out),
-            held(gate_cot),
-            held(right),
-            pltpu.SemaphoreType.DMA((3,)),
+            *[pltpu.VMEM(value.shape, value.dtype) for value in args],
+            pltpu.VMEM((rep, rows, block), F32),
+            pltpu.SemaphoreType.DMA((len(args),)),
+            pltpu.SemaphoreType.DMA((PIECES + 1,)),
         ],
         cost_estimate=pl.CostEstimate(
-            flops=flops, bytes_accessed=1 << 22, transcendentals=0
+            flops=2 * tokens * block * (width + block),
+            bytes_accessed=1 << 22,
+            transcendentals=0,
         ),
-    )(normed, rec_cot, conv_out, gate_cot, right)
+    )(*args)
 
 
 def middle_kernel(arrived, left, tiles):

time: 126 us -> 124 us (0.984)
  Pallas kernels: 8.45 us -> 6.78 us
    pallas_call x1, Pallas kernels: 5.85 us -> 4.18 us  [product(): pl.pallas_call(product_kernel, in_specs=[pl.BlockSpec(memory_space=pl.ANY...]
where the time goes in v6:
time: 124 us
  blocking collectives  105 us (85%)
  starting transfers between devices  9 us (7%)
  Pallas kernels  6.78 us (5%)
  waiting for transfers between devices  2.01 us (2%)
    all_to_all x3, blocking collectives, exchange(): return lax.all_to_all(tiles, axes, split_axis=0, concat_axis=0, tiled=True)  64.3 us
    all_gather x1, blocking collectives, shards(): lax.all_gather(gate_left[0].astype(F32), FS, tiled=True)  31.7 us
    all_gather x1, blocking collectives, shards(): full = lax.all_gather(mine, 'rep')  9.47 us
    all_to_all x2, starting transfers between devices, exchange(): return lax.all_to_all(tiles, axes, split_axis=0, concat_axis=0, tiled=True)  9 us
    pallas_call x1, Pallas kernels, product(): pl.pallas_call(product_kernel, in_specs=[pl.BlockSpec(memory_space=pl.ANY...  4.18 us
    pallas_call x5, Pallas kernels, on_core(): pl.pallas_call(kernel, out_shape=outs[0] if single else outs, in_specs=[w...  2.6 us
  transfers between devices with their start and end apart: 2, of which 1 were waited for; matrix products, arithmetic and copies ran while one was open for 0% of the time, Pallas kernels for 0%

profile of v6, /device:TPU:1, one launch (start us, length us, event | category | flops | bytes accessed | tf_op | source)
XLA Modules:
  0.0 124.0 jit_solution(1750407521530103528)
XLA Ops:
  0.6 4.2 %product.1 = f32[4,640,256]{2,1,0:T(8,128)} custom-call(bf16[640,2048]{1,0:T(8,128)(2,1)} %normed_hbm.1, bf16[640,256]{1,0:T(8,128)(2,1)} %cot_hbm.1, bf16[640,256]{1,0:T(8,128)(2,1)} %conv_hbm.1, bf16[640,256]{1,0:T(8,128)(2,1)} %gate_hbm.1, bf16[256,256]{1,0:T(8,128)(2,1)} %bitcast.18), custom_call_target="tpu_custom_call" | custom-call | flops 754974720 | bytes 4194304 | tf_op jit(solution)/shard_map/product/pallas_call | solution.py:136
  4.8 0.0 copy-start.5
  4.8 5.0 %all-to-all-start = ((f32[4,640,256]{2,1,0:T(8,128)}), f32[4,640,256]{2,1,0:T(8,128)S(1)}, u32[]{:S(2)}, u32[]{:S(2)}) async-start(f32[4,640,256]{2,1,0:T(8,128)} %product.1), calls=%async_computation | async-start | bytes 5242880 | tf_op jit(solution)/shard_map/near/all_to_all | solution.py:32
  9.8 0.0 copy-done.5
  9.9 31.7 %all-gather = f32[1,256,256]{2,1,0:T(8,128)S(1)} all-gather(f32[1,16,256]{2,1,0:T(8,128)S(1)} %convert_element_type.8), channel_id=2, replica_groups=mesh['fs_hi'=4,'fs_lo'=4,'rep'=4,'tp_0'=4,'tp_1'=2] {'fs_hi','fs_lo'}, dimensions={1}, use_global_device_ids=true | all-gather | bytes 278528 | tf_op jit(solution)/shard_map/left/all_gather | solution.py:358
  41.6 0.0 all-to-all-done.arrived
  41.6 0.0 copy-start
  41.6 0.0 copy-start.1
  41.6 0.0 copy-start.3
  41.6 0.4 middle.1
  42.0 0.0 copy-start.2
  42.0 0.0 copy-start.4
  42.0 20.5 %all_to_all.25.tiles = f32[4,160,256]{2,1,0:T(8,128)S(1)} all-to-all(f32[4,160,256]{2,1,0:T(8,128)S(1)} %bitcast.13), channel_id=1, replica_groups=mesh['fs_hi'=4,'fs_lo'=4,'rep'=4,'tp_0'=4,'tp_1'=2] {'fs_lo'}, dimensions={0} | all-to-all | bytes 1310720 | tf_op jit(solution)/shard_map/quarter/all_to_all | solution.py:32
  62.5 26.6 %all_to_all.26.arrived = f32[4,40,256]{2,1,0:T(8,128)S(1)} all-to-all(f32[4,40,256]{2,1,0:T(8,128)S(1)} %bitcast.14), channel_id=1, replica_groups=mesh['fs_hi'=4,'fs_lo'=4,'rep'=4,'tp_0'=4,'tp_1'=2] {'fs_hi'}, dimensions={0} | all-to-all | bytes 327680 | tf_op jit(solution)/shard_map/far/all_to_all | solution.py:32
  89.1 0.0 copy-done
  89.1 0.0 copy-done.1
  89.1 0.0 copy-done.3
  89.1 1.1 settle.1
  90.2 4.0 %all-to-all-start.3 = ((f32[16,4,128]{2,1,0:T(4,128)}), f32[16,4,128]{2,1,0:T(4,128)S(1)}, u32[]{:S(2)}, u32[]{:S(2)}) async-start(f32[16,4,128]{2,1,0:T(4,128)} %get-tuple-element.18), calls=%async_computation.3 | async-start | bytes 65536 | tf_op jit(solution)/shard_map/sums/all_to_all | solution.py:32
  94.2 9.5 %all-gather.1 = f32[160,256]{1,0:T(8,128)S(1)} all-gather(f32[40,256]{1,0:T(8,128)S(1)} %get-tuple-element.19), channel_id=3, replica_groups=mesh['fs_hi'=4,'fs_lo'=4,'rep'=4,'tp_0'=4,'tp_1'=2] {'rep'}, dimensions={0}, use_global_device_ids=true | all-gather | bytes 204800 | tf_op jit(solution)/shard_map/share/all_gather | solution.py:377
  103.7 2.0 %all-to-all-done.3.tiles = f32[16,4,128]{2,1,0:T(4,128)S(1)} async-done(((f32[16,4,128]{2,1,0:T(4,128)}), f32[16,4,128]{2,1,0:T(4,128)S(1)}, u32[]{:S(2)}, u32[]{:S(2)}) %all-to-all-start.3) | async-done | bytes 32800 | tf_op jit(solution)/shard_map/sums/all_to_all | solution.py:32
  105.7 17.2 %all_to_all.27.sums = f32[32,4,128]{2,1,0:T(4,128)S(1)} all-to-all(f32[32,4,128]{2,1,0:T(4,128)S(1)} %sums.1), channel_id=1, replica_groups=mesh['fs_hi'=4,'fs_lo'=4,'rep'=4,'tp_0'=4,'tp_1'=2] {'rep','tp_0','tp_1'}, dimensions={0} | all-to-all | bytes 131072 | tf_op jit(solution)/shard_map/sums/all_to_all | solution.py:32
  122.9 0.0 copy-done.2
  122.9 0.0 copy-done.4
  122.9 1.1 update.1
  (3 shorter events, 0.1 us)
Async XLA Ops:
  4.8 5.0 %copy-start.5 = (bf16[1,16,256]{2,1,0:T(8,128)(2,1)S(1)}, bf16[1,16,256]{2,1,0:T(8,128)(2,1)}, u32[]{:S(2)}) copy-start(bf16[1,16,256]{2,1,0:T(8,128)(2,1)} %param.20) | copy-start | bytes 24580
  4.8 36.7 %all-to-all-start = ((f32[4,640,256]{2,1,0:T(8,128)}), f32[4,640,256]{2,1,0:T(8,128)S(1)}, u32[]{:S(2)}, u32[]{:S(2)}) async-start(f32[4,640,256]{2,1,0:T(8,128)} %product.1), calls=%async_computation | async-start | bytes 5242880 | tf_op jit(solution)/shard_map/near/all_to_all | solution.py:32
  41.6 47.5 %copy-start = (bf16[256,256]{1,0:T(8,128)(2,1)S(1)}, bf16[256,256]{1,0:T(8,128)(2,1)}, u32[]{:S(2)}) copy-start(bf16[256,256]{1,0:T(8,128)(2,1)} %rec_right.1) | copy-start | bytes 393220
  41.6 47.5 %copy-start.1 = (f32[128,256]{1,0:T(8,128)S(1)}, f32[128,256]{1,0:T(8,128)}, u32[]{:S(2)}) copy-start(f32[128,256]{1,0:T(8,128)} %rec_moment.1) | copy-start | bytes 393220
  41.6 47.5 %copy-start.3 = (f32[1,16,256]{2,1,0:T(8,128)S(1)}, f32[1,16,256]{2,1,0:T(8,128)}, u32[]{:S(2)}) copy-start(f32[1,16,256]{2,1,0:T(8,128)} %param.19) | copy-start | bytes 49156
  42.0 81.0 %copy-start.2 = (f32[128,256]{1,0:T(8,128)S(1)}, f32[128,256]{1,0:T(8,128)}, u32[]{:S(2)}) copy-start(f32[128,256]{1,0:T(8,128)} %rec_weight.1) | copy-start | bytes 393220
  42.0 81.0 %copy-start.4 = (f32[1,16,256]{2,1,0:T(8,128)S(1)}, f32[1,16,256]{2,1,0:T(8,128)}, u32[]{:S(2)}) copy-start(f32[1,16,256]{2,1,0:T(8,128)} %param.18) | copy-start | bytes 49156
  90.2 15.5 %all-to-all-start.3 = ((f32[16,4,128]{2,1,0:T(4,128)}), f32[16,4,128]{2,1,0:T(4,128)S(1)}, u32[]{:S(2)}, u32[]{:S(2)}) async-start(f32[16,4,128]{2,1,0:T(4,128)} %get-tuple-element.18), calls=%async_computation.3 | async-start | bytes 65536 | tf_op jit(solution)/shard_map/sums/all_to_all | solution.py:32

commit v7 on v6

--- a/solution.py
+++ b/solution.py
@@ -6,7 +6,8 @@
 from jax.sharding import Mesh
 from jax.sharding import PartitionSpec as P
 
-FS = ("fs_hi", "fs_lo")
+CORE = ("fs", "tp_1")
+QUARTER = 4
 TP = ("tp_0", "tp_1")
 
 BETA = 0.9
@@ -28,8 +29,31 @@
     return size
 
 
-def exchange(tiles, axes):
-    return lax.all_to_all(tiles, axes, split_axis=0, concat_axis=0, tiled=True)
+def exchange(tiles, axes, groups=None):
+    return lax.all_to_all(
+        tiles,
+        axes,
+        split_axis=0,
+        concat_axis=0,
+        tiled=True,
+        axis_index_groups=groups,
+    )
+
+
+def chip_at(hi, lo, core, fs):
+    return (hi * QUARTER + lo + core * (QUARTER // 2)) % fs
+
+
+def z_groups(fs, cores, within):
+    hi, lo = fs // QUARTER, QUARTER
+    place = lambda h, l, c: chip_at(h, l, c, fs) * cores + c
+    if within:
+        return [
+            [place(h, l, c) for l in range(lo)] for h in range(hi) for c in range(cores)
+        ]
+    return [
+        [place(h, l, c) for h in range(hi)] for l in range(lo) for c in range(cores)
+    ]
 
 
 def whole():
@@ -165,8 +189,12 @@
             value += arrived[r, pl.ds(start, size), :]
         return value
 
-    lo = lax.axis_size("fs_lo")
-    place = [f % lo * (fs // lo) + f // lo for f in range(fs)]
+    core = lax.axis_index("tp_1")
+    hi = fs // QUARTER
+    place = []
+    for f in range(fs):
+        at = lax.rem(f + fs - core * (QUARTER // 2), fs)
+        place.append(lax.rem(at, QUARTER) * hi + lax.div(at, QUARTER))
     for f in range(fs):
         tiles[place[f], pl.ds(0, run), :] = total(f * run, run)
     turned = total(rec_rows, share)
@@ -346,7 +374,7 @@
     gate_left,
     gate_right,
 ):
-    fs, rep = size_of(FS), lax.axis_size("rep")
+    fs, rep = lax.axis_size("fs"), lax.axis_size("rep")
     like = lambda value, kind=F32: jax.ShapeDtypeStruct(value.shape, kind)
     gate_weight, gate_moment = gate_weight[0], gate_moment[0]
 
@@ -355,15 +383,17 @@
     with jax.named_scope("near"):
         arrived = exchange(tiles, "rep")
     with jax.named_scope("left"):
-        left = lax.all_gather(gate_left[0].astype(F32), FS, tiled=True).reshape(fs, *gate_left.shape[1:])
+        left = lax.all_gather(gate_left[0].astype(F32), "fs", tiled=True).reshape(fs, *gate_left.shape[1:])
     with jax.named_scope("middle"):
         tiles = middle(arrived, left)
     with jax.named_scope("quarter"):
-        hi, lo = lax.axis_size("fs_hi"), lax.axis_size("fs_lo")
+        hi, lo, cores = fs // QUARTER, QUARTER, lax.axis_size("tp_1")
         rows = tiles.shape[1]
-        tiles = add_up(exchange(tiles.reshape(lo, hi * rows, -1), "fs_lo"))
+        tiles = tiles.reshape(lo, hi * rows, -1)
+        tiles = add_up(exchange(tiles, CORE, z_groups(fs, cores, True)))
     with jax.named_scope("far"):
-        arrived = exchange(tiles.reshape(hi, rows, -1), "fs_hi")
+        tiles = tiles.reshape(hi, rows, -1)
+        arrived = exchange(tiles, CORE, z_groups(fs, cores, False))
     with jax.named_scope("settle"):
         mine, sums = on_core(
             settle_kernel,
@@ -376,7 +406,7 @@
     with jax.named_scope("share"):
         full = lax.all_gather(mine, "rep")
     with jax.named_scope("sums"):
-        sums = fold(exchange(sums, FS), rep * size_of(TP), full)
+        sums = fold(exchange(sums, "fs"), rep * size_of(TP), full)
         sums = exchange(sums, ("rep", *TP))
     with jax.named_scope("update"):
         bf16 = jnp.bfloat16
@@ -418,21 +448,21 @@
 def solution(mesh):
     fs, rep, tp = (mesh.shape[name] for name in ("fs", "rep", "tp"))
     split = Mesh(
-        mesh.devices.reshape(fs // 4, 4, rep, tp // 2, 2),
-        (*FS, "rep", *TP),
-    )
-    tokens = (*FS, "rep")
+        mesh.devices.reshape(fs, rep, tp // 2, 2),
+        ("fs", "rep", *TP),
+    )
+    tokens = ("fs", "rep")
     placed = (
         P(tokens, None),
         P(tokens, TP),
         P(tokens, TP),
         P(tokens, TP),
-        P(FS, TP),
-        P(FS, TP),
+        P("fs", TP),
+        P("fs", TP),
         P(TP, None),
-        P(TP, FS, None),
-        P(TP, FS, None),
-        P(TP, FS, None),
+        P(TP, "fs", None),
+        P(TP, "fs", None),
+        P(TP, "fs", None),
         P(TP, None, None),
     )
 
@@ -440,6 +470,6 @@
         shards,
         mesh=split,
         in_specs=placed,
-        out_specs=(P(FS, TP),) * 4 + (P(TP, FS, None),) * 4,
+        out_specs=(P("fs", TP),) * 4 + (P(TP, "fs", None),) * 4,
         check_vma=False,
     )

time: 124 us -> 122 us (0.984)
  blocking collectives: 105 us -> 97.2 us
  starting transfers between devices: 9 us -> 15.5 us
    all_to_all x3, blocking collectives: 64.3 us -> 55.7 us  [exchange(): lax.all_to_all(tiles, axes, split_axis=0, concat_axis=0, tiled=True, axis...]
    all_to_all x2, starting transfers between devices: 9 us -> 15.5 us  [exchange(): lax.all_to_all(tiles, axes, split_axis=0, concat_axis=0, tiled=True, axis...]
where the time goes in v7:
time: 122 us
  blocking collectives  97.2 us (80%)
  starting transfers between devices  15.5 us (13%)
  Pallas kernels  6.81 us (6%)
  waiting for transfers between devices  1.71 us (1%)
    all_to_all x3, blocking collectives, exchange(): lax.all_to_all(tiles, axes, split_axis=0, concat_axis=0, tiled=True, axis...  55.7 us
    all_gather x1, blocking collectives, shards(): lax.all_gather(gate_left[0].astype(F32), 'fs', tiled=True)  31.7 us
    all_to_all x2, starting transfers between devices, exchange(): lax.all_to_all(tiles, axes, split_axis=0, concat_axis=0, tiled=True, axis...  15.5 us
    all_gather x1, blocking collectives, shards(): full = lax.all_gather(mine, 'rep')  9.76 us
    pallas_call x1, Pallas kernels, product(): pl.pallas_call(product_kernel, in_specs=[pl.BlockSpec(memory_space=pl.ANY...  4.18 us
    pallas_call x5, Pallas kernels, on_core(): pl.pallas_call(kernel, out_shape=outs[0] if single else outs, in_specs=[w...  2.63 us
  transfers between devices with their start and end apart: 2, of which 1 were waited for; matrix products, arithmetic and copies ran while one was open for 0% of the time, Pallas kernels for 0%

profile of v7, /device:TPU:1, one launch (start us, length us, event | category | flops | bytes accessed | tf_op | source)
XLA Modules:
  0.0 122.0 jit_solution(9462101729417826539)
XLA Ops:
  0.6 4.2 %product.1 = f32[4,640,256]{2,1,0:T(8,128)} custom-call(bf16[640,2048]{1,0:T(8,128)(2,1)} %normed_hbm.1, bf16[640,256]{1,0:T(8,128)(2,1)} %cot_hbm.1, bf16[640,256]{1,0:T(8,128)(2,1)} %conv_hbm.1, bf16[640,256]{1,0:T(8,128)(2,1)} %gate_hbm.1, bf16[256,256]{1,0:T(8,128)(2,1)} %bitcast.18), custom_call_target="tpu_custom_call" | custom-call | flops 754974720 | bytes 4194304 | tf_op jit(solution)/shard_map/product/pallas_call | solution.py:160
  4.8 0.0 copy-start.5
  4.8 5.0 %all-to-all-start = ((f32[4,640,256]{2,1,0:T(8,128)}), f32[4,640,256]{2,1,0:T(8,128)S(1)}, u32[]{:S(2)}, u32[]{:S(2)}) async-start(f32[4,640,256]{2,1,0:T(8,128)} %product.1), calls=%async_computation | async-start | bytes 5242880 | tf_op jit(solution)/shard_map/near/all_to_all | solution.py:33
  9.8 0.0 copy-done.5
  9.9 31.7 %all-gather = f32[1,256,256]{2,1,0:T(8,128)S(1)} all-gather(f32[1,16,256]{2,1,0:T(8,128)S(1)} %convert_element_type.8), channel_id=2, replica_groups=mesh['fs'=16,'rep'=4,'tp_0'=4,'tp_1'=2] {'fs'}, dimensions={1}, use_global_device_ids=true | all-gather | bytes 278528 | tf_op jit(solution)/shard_map/left/all_gather | solution.py:386
  41.6 0.0 all-to-all-done.arrived
  41.6 0.0 copy-start
  41.6 0.0 copy-start.1
  41.6 0.0 copy-start.3
  41.6 0.4 middle.1
  42.0 0.0 copy-start.2
  42.0 0.0 copy-start.4
  42.0 21.8 %all_to_all.25.tiles = f32[4,160,256]{2,1,0:T(8,128)S(1)} all-to-all(f32[4,160,256]{2,1,0:T(8,128)S(1)} %bitcast.13), channel_id=1, replica_groups={{0,32,64,96},{65,97,129,161},{128,160,192,224},{193,225,257,289},{256,2..., dimensions={0} | all-to-all | bytes 1310720 | tf_op jit(solution)/shard_map/quarter/all_to_all | solution.py:33
  63.9 19.6 %all_to_all.26.arrived = f32[4,40,256]{2,1,0:T(8,128)S(1)} all-to-all(f32[4,40,256]{2,1,0:T(8,128)S(1)} %bitcast.14), channel_id=1, replica_groups={{0,128,256,384},{65,193,321,449},{32,160,288,416},{97,225,353,481},{64,..., dimensions={0} | all-to-all | bytes 327680 | tf_op jit(solution)/shard_map/far/all_to_all | solution.py:33
  83.5 0.0 copy-done
  83.5 0.0 copy-done.1
  83.5 0.0 copy-done.3
  83.5 1.1 settle.1
  84.6 10.5 %all-to-all-start.3 = ((f32[16,4,128]{2,1,0:T(4,128)}), f32[16,4,128]{2,1,0:T(4,128)S(1)}, u32[]{:S(2)}, u32[]{:S(2)}) async-start(f32[16,4,128]{2,1,0:T(4,128)} %get-tuple-element.18), calls=%async_computation.3 | async-start | bytes 65536 | tf_op jit(solution)/shard_map/sums/all_to_all | solution.py:33
  95.1 9.8 %all-gather.1 = f32[160,256]{1,0:T(8,128)S(1)} all-gather(f32[40,256]{1,0:T(8,128)S(1)} %get-tuple-element.19), channel_id=3, replica_groups=mesh['fs'=16,'rep'=4,'tp_0'=4,'tp_1'=2] {'rep'}, dimensions={0}, use_global_device_ids=true | all-gather | bytes 204800 | tf_op jit(solution)/shard_map/share/all_gather | solution.py:407
  104.9 1.7 %all-to-all-done.3.tiles = f32[16,4,128]{2,1,0:T(4,128)S(1)} async-done(((f32[16,4,128]{2,1,0:T(4,128)}), f32[16,4,128]{2,1,0:T(4,128)S(1)}, u32[]{:S(2)}, u32[]{:S(2)}) %all-to-all-start.3) | async-done | bytes 32800 | tf_op jit(solution)/shard_map/sums/all_to_all | solution.py:33
  106.6 14.2 %all_to_all.27.sums = f32[32,4,128]{2,1,0:T(4,128)S(1)} all-to-all(f32[32,4,128]{2,1,0:T(4,128)S(1)} %sums.1), channel_id=1, replica_groups=mesh['fs'=16,'rep'=4,'tp_0'=4,'tp_1'=2] {'rep','tp_0','tp_1'}, dimensions={0} | all-to-all | bytes 131072 | tf_op jit(solution)/shard_map/sums/all_to_all | solution.py:33
  120.9 0.0 copy-done.2
  120.9 0.0 copy-done.4
  120.9 1.1 update.1
  (3 shorter events, 0.1 us)
Async XLA Ops:
  4.8 5.0 %copy-start.5 = (bf16[1,16,256]{2,1,0:T(8,128)(2,1)S(1)}, bf16[1,16,256]{2,1,0:T(8,128)(2,1)}, u32[]{:S(2)}) copy-start(bf16[1,16,256]{2,1,0:T(8,128)(2,1)} %param.20) | copy-start | bytes 24580
  4.8 36.7 %all-to-all-start = ((f32[4,640,256]{2,1,0:T(8,128)}), f32[4,640,256]{2,1,0:T(8,128)S(1)}, u32[]{:S(2)}, u32[]{:S(2)}) async-start(f32[4,640,256]{2,1,0:T(8,128)} %product.1), calls=%async_computation | async-start | bytes 5242880 | tf_op jit(solution)/shard_map/near/all_to_all | solution.py:33
  41.6 41.9 %copy-start = (bf16[256,256]{1,0:T(8,128)(2,1)S(1)}, bf16[256,256]{1,0:T(8,128)(2,1)}, u32[]{:S(2)}) copy-start(bf16[256,256]{1,0:T(8,128)(2,1)} %rec_right.1) | copy-start | bytes 393220
  41.6 41.9 %copy-start.1 = (f32[128,256]{1,0:T(8,128)S(1)}, f32[128,256]{1,0:T(8,128)}, u32[]{:S(2)}) copy-start(f32[128,256]{1,0:T(8,128)} %rec_moment.1) | copy-start | bytes 393220
  41.6 42.0 %copy-start.3 = (f32[1,16,256]{2,1,0:T(8,128)S(1)}, f32[1,16,256]{2,1,0:T(8,128)}, u32[]{:S(2)}) copy-start(f32[1,16,256]{2,1,0:T(8,128)} %param.19) | copy-start | bytes 49156
  42.0 78.9 %copy-start.2 = (f32[128,256]{1,0:T(8,128)S(1)}, f32[128,256]{1,0:T(8,128)}, u32[]{:S(2)}) copy-start(f32[128,256]{1,0:T(8,128)} %rec_weight.1) | copy-start | bytes 393220
  42.0 78.9 %copy-start.4 = (f32[1,16,256]{2,1,0:T(8,128)S(1)}, f32[1,16,256]{2,1,0:T(8,128)}, u32[]{:S(2)}) copy-start(f32[1,16,256]{2,1,0:T(8,128)} %param.18) | copy-start | bytes 49156
  84.6 22.0 %all-to-all-start.3 = ((f32[16,4,128]{2,1,0:T(4,128)}), f32[16,4,128]{2,1,0:T(4,128)S(1)}, u32[]{:S(2)}, u32[]{:S(2)}) async-start(f32[16,4,128]{2,1,0:T(4,128)} %get-tuple-element.18), calls=%async_computation.3 | async-start | bytes 65536 | tf_op jit(solution)/shard_map/sums/all_to_all | solution.py:33

commit v8 on v7

--- a/solution.py
+++ b/solution.py
@@ -7,7 +7,7 @@
 from jax.sharding import PartitionSpec as P
 
 CORE = ("fs", "tp_1")
-QUARTER = 4
+SPAN = 2
 TP = ("tp_0", "tp_1")
 
 BETA = 0.9
@@ -41,11 +41,11 @@
 
 
 def chip_at(hi, lo, core, fs):
-    return (hi * QUARTER + lo + core * (QUARTER // 2)) % fs
+    return (hi * SPAN + lo + core * (SPAN // 2)) % fs
 
 
 def z_groups(fs, cores, within):
-    hi, lo = fs // QUARTER, QUARTER
+    hi, lo = fs // SPAN, SPAN
     place = lambda h, l, c: chip_at(h, l, c, fs) * cores + c
     if within:
         return [
@@ -190,11 +190,11 @@
         return value
 
     core = lax.axis_index("tp_1")
-    hi = fs // QUARTER
+    hi = fs // SPAN
     place = []
     for f in range(fs):
-        at = lax.rem(f + fs - core * (QUARTER // 2), fs)
-        place.append(lax.rem(at, QUARTER) * hi + lax.div(at, QUARTER))
+        at = lax.rem(f + fs - core * (SPAN // 2), fs)
+        place.append(lax.rem(at, SPAN) * hi + lax.div(at, SPAN))
     for f in range(fs):
         tiles[place[f], pl.ds(0, run), :] = total(f * run, run)
     turned = total(rec_rows, share)
@@ -387,7 +387,7 @@
     with jax.named_scope("middle"):
         tiles = middle(arrived, left)
     with jax.named_scope("quarter"):
-        hi, lo, cores = fs // QUARTER, QUARTER, lax.axis_size("tp_1")
+        hi, lo, cores = fs // SPAN, SPAN, lax.axis_size("tp_1")
         rows = tiles.shape[1]
         tiles = tiles.reshape(lo, hi * rows, -1)
         tiles = add_up(exchange(tiles, CORE, z_groups(fs, cores, True)))

time: 122 us -> 121 us (level)
  starting transfers between devices: 15.5 us -> 13.1 us
    all_to_all x2, starting transfers between devices: 15.5 us -> 13.1 us  [exchange(): lax.all_to_all(tiles, axes, split_axis=0, concat_axis=0, tiled=True, axis...]
where the time goes in v8:
time: 121 us; the launch traced here: 120 us
  blocking collectives  98 us (81%)
  starting transfers between devices  13.1 us (11%)
  Pallas kernels  6.81 us (6%)
  waiting for transfers between devices  1.64 us (1%)
    all_to_all x3, blocking collectives, exchange(): lax.all_to_all(tiles, axes, split_axis=0, concat_axis=0, tiled=True, axis...  56.3 us
    all_gather x1, blocking collectives, shards(): lax.all_gather(gate_left[0].astype(F32), 'fs', tiled=True)  31.7 us
    all_to_all x2, starting transfers between devices, exchange(): lax.all_to_all(tiles, axes, split_axis=0, concat_axis=0, tiled=True, axis...  13.1 us
    all_gather x1, blocking collectives, shards(): full = lax.all_gather(mine, 'rep')  9.94 us
    pallas_call x1, Pallas kernels, product(): pl.pallas_call(product_kernel, in_specs=[pl.BlockSpec(memory_space=pl.ANY...  4.18 us
    pallas_call x5, Pallas kernels, on_core(): pl.pallas_call(kernel, out_shape=outs[0] if single else outs, in_specs=[w...  2.63 us
  transfers between devices with their start and end apart: 2, of which 1 were waited for; matrix products, arithmetic and copies ran while one was open for 0% of the time, Pallas kernels for 0%

profile of v8, /device:TPU:1, one launch (start us, length us, event | category | flops | bytes accessed | tf_op | source)
XLA Modules:
  0.0 120.2 jit_solution(15012470769250382191)
XLA Ops:
  0.6 4.2 %product.1 = f32[4,640,256]{2,1,0:T(8,128)} custom-call(bf16[640,2048]{1,0:T(8,128)(2,1)} %normed_hbm.1, bf16[640,256]{1,0:T(8,128)(2,1)} %cot_hbm.1, bf16[640,256]{1,0:T(8,128)(2,1)} %conv_hbm.1, bf16[640,256]{1,0:T(8,128)(2,1)} %gate_hbm.1, bf16[256,256]{1,0:T(8,128)(2,1)} %bitcast.18), custom_call_target="tpu_custom_call" | custom-call | flops 754974720 | bytes 4194304 | tf_op jit(solution)/shard_map/product/pallas_call | solution.py:160
  4.8 0.0 copy-start.5
  4.8 5.0 %all-to-all-start = ((f32[4,640,256]{2,1,0:T(8,128)}), f32[4,640,256]{2,1,0:T(8,128)S(1)}, u32[]{:S(2)}, u32[]{:S(2)}) async-start(f32[4,640,256]{2,1,0:T(8,128)} %product.1), calls=%async_computation | async-start | bytes 5242880 | tf_op jit(solution)/shard_map/near/all_to_all | solution.py:33
  9.8 0.0 copy-done.5
  9.9 31.7 %all-gather = f32[1,256,256]{2,1,0:T(8,128)S(1)} all-gather(f32[1,16,256]{2,1,0:T(8,128)S(1)} %convert_element_type.8), channel_id=2, replica_groups=mesh['fs'=16,'rep'=4,'tp_0'=4,'tp_1'=2] {'fs'}, dimensions={1}, use_global_device_ids=true | all-gather | bytes 278528 | tf_op jit(solution)/shard_map/left/all_gather | solution.py:386
  41.6 0.0 all-to-all-done.arrived
  41.6 0.0 copy-start
  41.6 0.0 copy-start.1
  41.6 0.0 copy-start.3
  41.6 0.4 middle.1
  42.0 0.0 copy-start.2
  42.0 0.0 copy-start.4
  42.0 15.8 %all_to_all.25.tiles = f32[2,320,256]{2,1,0:T(8,128)S(1)} all-to-all(f32[2,320,256]{2,1,0:T(8,128)S(1)} %bitcast.14), channel_id=1, replica_groups={{0,32},{33,65},{64,96},{97,129},{128,160},{161,193},{192,224},{225,257}..., dimensions={0} | all-to-all | bytes 1310720 | tf_op jit(solution)/shard_map/quarter/all_to_all | solution.py:33
  57.8 24.9 %all_to_all.26.arrived = f32[8,40,256]{2,1,0:T(8,128)S(1)} all-to-all(f32[8,40,256]{2,1,0:T(8,128)S(1)} %bitcast.13), channel_id=1, replica_groups={{0,64,128,192,256,320,384,448},{33,97,161,225,289,353,417,481},{32,96,1..., dimensions={0} | all-to-all | bytes 655360 | tf_op jit(solution)/shard_map/far/all_to_all | solution.py:33
  82.7 0.0 copy-done
  82.7 0.0 copy-done.1
  82.7 0.0 copy-done.3
  82.7 1.1 settle.1
  83.9 8.1 %all-to-all-start.3 = ((f32[16,4,128]{2,1,0:T(4,128)}), f32[16,4,128]{2,1,0:T(4,128)S(1)}, u32[]{:S(2)}, u32[]{:S(2)}) async-start(f32[16,4,128]{2,1,0:T(4,128)} %get-tuple-element.18), calls=%async_computation.3 | async-start | bytes 65536 | tf_op jit(solution)/shard_map/sums/all_to_all | solution.py:33
  91.9 9.9 %all-gather.1 = f32[160,256]{1,0:T(8,128)S(1)} all-gather(f32[40,256]{1,0:T(8,128)S(1)} %get-tuple-element.19), channel_id=3, replica_groups=mesh['fs'=16,'rep'=4,'tp_0'=4,'tp_1'=2] {'rep'}, dimensions={0}, use_global_device_ids=true | all-gather | bytes 204800 | tf_op jit(solution)/shard_map/share/all_gather | solution.py:407
  101.9 1.6 %all-to-all-done.3.tiles = f32[16,4,128]{2,1,0:T(4,128)S(1)} async-done(((f32[16,4,128]{2,1,0:T(4,128)}), f32[16,4,128]{2,1,0:T(4,128)S(1)}, u32[]{:S(2)}, u32[]{:S(2)}) %all-to-all-start.3) | async-done | bytes 32800 | tf_op jit(solution)/shard_map/sums/all_to_all | solution.py:33
  103.5 15.6 %all_to_all.27.sums = f32[32,4,128]{2,1,0:T(4,128)S(1)} all-to-all(f32[32,4,128]{2,1,0:T(4,128)S(1)} %sums.1), channel_id=1, replica_groups=mesh['fs'=16,'rep'=4,'tp_0'=4,'tp_1'=2] {'rep','tp_0','tp_1'}, dimensions={0} | all-to-all | bytes 131072 | tf_op jit(solution)/shard_map/sums/all_to_all | solution.py:33
  119.1 0.0 copy-done.2
  119.1 0.0 copy-done.4
  119.2 1.1 update.1
  (3 shorter events, 0.1 us)
Async XLA Ops:
  4.8 5.0 %copy-start.5 = (bf16[1,16,256]{2,1,0:T(8,128)(2,1)S(1)}, bf16[1,16,256]{2,1,0:T(8,128)(2,1)}, u32[]{:S(2)}) copy-start(bf16[1,16,256]{2,1,0:T(8,128)(2,1)} %param.20) | copy-start | bytes 24580
  4.8 36.7 %all-to-all-start = ((f32[4,640,256]{2,1,0:T(8,128)}), f32[4,640,256]{2,1,0:T(8,128)S(1)}, u32[]{:S(2)}, u32[]{:S(2)}) async-start(f32[4,640,256]{2,1,0:T(8,128)} %product.1), calls=%async_computation | async-start | bytes 5242880 | tf_op jit(solution)/shard_map/near/all_to_all | solution.py:33
  41.6 41.2 %copy-start = (bf16[256,256]{1,0:T(8,128)(2,1)S(1)}, bf16[256,256]{1,0:T(8,128)(2,1)}, u32[]{:S(2)}) copy-start(bf16[256,256]{1,0:T(8,128)(2,1)} %rec_right.1) | copy-start | bytes 393220
  41.6 41.2 %copy-start.1 = (f32[128,256]{1,0:T(8,128)S(1)}, f32[128,256]{1,0:T(8,128)}, u32[]{:S(2)}) copy-start(f32[128,256]{1,0:T(8,128)} %rec_moment.1) | copy-start | bytes 393220
  41.6 41.2 %copy-start.3 = (f32[1,16,256]{2,1,0:T(8,128)S(1)}, f32[1,16,256]{2,1,0:T(8,128)}, u32[]{:S(2)}) copy-start(f32[1,16,256]{2,1,0:T(8,128)} %param.19) | copy-start | bytes 49156
  42.0 77.2 %copy-start.2 = (f32[128,256]{1,0:T(8,128)S(1)}, f32[128,256]{1,0:T(8,128)}, u32[]{:S(2)}) copy-start(f32[128,256]{1,0:T(8,128)} %rec_weight.1) | copy-start | bytes 393220
  42.0 77.2 %copy-start.4 = (f32[1,16,256]{2,1,0:T(8,128)S(1)}, f32[1,16,256]{2,1,0:T(8,128)}, u32[]{:S(2)}) copy-start(f32[1,16,256]{2,1,0:T(8,128)} %param.18) | copy-start | bytes 49156
  83.9 19.7 %all-to-all-start.3 = ((f32[16,4,128]{2,1,0:T(4,128)}), f32[16,4,128]{2,1,0:T(4,128)S(1)}, u32[]{:S(2)}, u32[]{:S(2)}) async-start(f32[16,4,128]{2,1,0:T(4,128)} %get-tuple-element.18), calls=%async_computation.3 | async-start | bytes 65536 | tf_op jit(solution)/shard_map/sums/all_to_all | solution.py:33

commit v9 on v8

--- a/solution.py
+++ b/solution.py
@@ -7,6 +7,7 @@
 from jax.sharding import PartitionSpec as P
 
 CORE = ("fs", "tp_1")
+PLANE = ("rep", "tp_0")
 SPAN = 2
 TP = ("tp_0", "tp_1")
 
@@ -399,15 +400,15 @@
             settle_kernel,
             (
                 jax.ShapeDtypeStruct(arrived.shape[1:], F32),
-                jax.ShapeDtypeStruct((fs, 4, 128), F32),
+                jax.ShapeDtypeStruct((size_of(CORE), 4, 128), F32),
             ),
             (arrived, rec_right, rec_moment, gate_moment),
         )
     with jax.named_scope("share"):
         full = lax.all_gather(mine, "rep")
     with jax.named_scope("sums"):
-        sums = fold(exchange(sums, "fs"), rep * size_of(TP), full)
-        sums = exchange(sums, ("rep", *TP))
+        sums = fold(exchange(sums, CORE), size_of(PLANE), full)
+        sums = exchange(sums, PLANE)
     with jax.named_scope("update"):
         bf16 = jnp.bfloat16
         (

time: 121 us -> 121 us (level)
  blocking collectives: 98 us -> 93.4 us
  starting transfers between devices: 13.1 us -> 15.5 us
  waiting for transfers between devices: 1.64 us -> 2.96 us
    all_to_all x3, blocking collectives: 56.3 us -> 51.7 us  [exchange(): lax.all_to_all(tiles, axes, split_axis=0, concat_axis=0, tiled=True, axis...]
    all_to_all x2, starting transfers between devices: 13.1 us -> 15.5 us  [exchange(): lax.all_to_all(tiles, axes, split_axis=0, concat_axis=0, tiled=True, axis...]
    all_to_all x2, waiting for transfers between devices: 1.64 us -> 2.96 us  [exchange(): lax.all_to_all(tiles, axes, split_axis=0, concat_axis=0, tiled=True, axis...]
where the time goes in v9:
time: 121 us; the launch traced here: 119 us
  blocking collectives  93.4 us (77%)
  starting transfers between devices  15.5 us (13%)
  Pallas kernels  6.84 us (6%)
  waiting for transfers between devices  2.96 us (2%)
    all_to_all x3, blocking collectives, exchange(): lax.all_to_all(tiles, axes, split_axis=0, concat_axis=0, tiled=True, axis...  51.7 us
    all_gather x1, blocking collectives, shards(): lax.all_gather(gate_left[0].astype(F32), 'fs', tiled=True)  31.7 us
    all_to_all x2, starting transfers between devices, exchange(): lax.all_to_all(tiles, axes, split_axis=0, concat_axis=0, tiled=True, axis...  15.5 us
    all_gather x1, blocking collectives, shards(): full = lax.all_gather(mine, 'rep')  10.1 us
    pallas_call x1, Pallas kernels, product(): pl.pallas_call(product_kernel, in_specs=[pl.BlockSpec(memory_space=pl.ANY...  4.18 us
    all_to_all x2, waiting for transfers between devices, exchange(): lax.all_to_all(tiles, axes, split_axis=0, concat_axis=0, tiled=True, axis...  2.96 us
    pallas_call x5, Pallas kernels, on_core(): pl.pallas_call(kernel, out_shape=outs[0] if single else outs, in_specs=[w...  2.66 us
  transfers between devices with their start and end apart: 2, of which 1 were waited for; matrix products, arithmetic and copies ran while one was open for 0% of the time, Pallas kernels for 0%

profile of v9, /device:TPU:1, one launch (start us, length us, event | category | flops | bytes accessed | tf_op | source)
XLA Modules:
  0.0 119.5 jit_solution(14548690490945045352)
XLA Ops:
  0.6 4.2 %product.1 = f32[4,640,256]{2,1,0:T(8,128)} custom-call(bf16[640,2048]{1,0:T(8,128)(2,1)} %normed_hbm.1, bf16[640,256]{1,0:T(8,128)(2,1)} %cot_hbm.1, bf16[640,256]{1,0:T(8,128)(2,1)} %conv_hbm.1, bf16[640,256]{1,0:T(8,128)(2,1)} %gate_hbm.1, bf16[256,256]{1,0:T(8,128)(2,1)} %bitcast.18), custom_call_target="tpu_custom_call" | custom-call | flops 754974720 | bytes 4194304 | tf_op jit(solution)/shard_map/product/pallas_call | solution.py:161
  4.8 0.0 copy-start.5
  4.8 5.0 %all-to-all-start = ((f32[4,640,256]{2,1,0:T(8,128)}), f32[4,640,256]{2,1,0:T(8,128)S(1)}, u32[]{:S(2)}, u32[]{:S(2)}) async-start(f32[4,640,256]{2,1,0:T(8,128)} %product.1), calls=%async_computation | async-start | bytes 5242880 | tf_op jit(solution)/shard_map/near/all_to_all | solution.py:34
  9.8 0.0 copy-done.5
  9.9 31.7 %all-gather = f32[1,256,256]{2,1,0:T(8,128)S(1)} all-gather(f32[1,16,256]{2,1,0:T(8,128)S(1)} %convert_element_type.8), channel_id=2, replica_groups=mesh['fs'=16,'rep'=4,'tp_0'=4,'tp_1'=2] {'fs'}, dimensions={1}, use_global_device_ids=true | all-gather | bytes 278528 | tf_op jit(solution)/shard_map/left/all_gather | solution.py:387
  41.6 0.0 all-to-all-done.arrived
  41.6 0.0 copy-start
  41.6 0.0 copy-start.1
  41.6 0.0 copy-start.3
  41.6 0.4 middle.1
  42.0 0.0 copy-start.2
  42.0 0.0 copy-start.4
  42.0 15.8 %all_to_all.25.tiles = f32[2,320,256]{2,1,0:T(8,128)S(1)} all-to-all(f32[2,320,256]{2,1,0:T(8,128)S(1)} %bitcast.14), channel_id=1, replica_groups={{0,32},{33,65},{64,96},{97,129},{128,160},{161,193},{192,224},{225,257}..., dimensions={0} | all-to-all | bytes 1310720 | tf_op jit(solution)/shard_map/quarter/all_to_all | solution.py:34
  57.8 24.9 %all_to_all.26.arrived = f32[8,40,256]{2,1,0:T(8,128)S(1)} all-to-all(f32[8,40,256]{2,1,0:T(8,128)S(1)} %bitcast.13), channel_id=1, replica_groups={{0,64,128,192,256,320,384,448},{33,97,161,225,289,353,417,481},{32,96,1..., dimensions={0} | all-to-all | bytes 655360 | tf_op jit(solution)/shard_map/far/all_to_all | solution.py:34
  82.7 0.0 copy-done
  82.7 0.0 copy-done.1
  82.7 0.0 copy-done.3
  82.7 1.1 settle.1
  83.9 10.5 %all-to-all-start.3 = ((f32[32,4,128]{2,1,0:T(4,128)}), f32[32,4,128]{2,1,0:T(4,128)S(1)}, u32[]{:S(2)}, u32[]{:S(2)}) async-start(f32[32,4,128]{2,1,0:T(4,128)} %get-tuple-element.18), calls=%async_computation.3 | async-start | bytes 131072 | tf_op jit(solution)/shard_map/sums/all_to_all | solution.py:34
  94.4 10.1 %all-gather.1 = f32[160,256]{1,0:T(8,128)S(1)} all-gather(f32[40,256]{1,0:T(8,128)S(1)} %get-tuple-element.19), channel_id=3, replica_groups=mesh['fs'=16,'rep'=4,'tp_0'=4,'tp_1'=2] {'rep'}, dimensions={0}, use_global_device_ids=true | all-gather | bytes 204800 | tf_op jit(solution)/shard_map/share/all_gather | solution.py:408
  104.4 3.0 %all-to-all-done.3.tiles = f32[32,4,128]{2,1,0:T(4,128)S(1)} async-done(((f32[32,4,128]{2,1,0:T(4,128)}), f32[32,4,128]{2,1,0:T(4,128)S(1)}, u32[]{:S(2)}, u32[]{:S(2)}) %all-to-all-start.3) | async-done | bytes 65568 | tf_op jit(solution)/shard_map/sums/all_to_all | solution.py:34
  107.4 11.0 %all_to_all.27.sums = f32[16,4,128]{2,1,0:T(4,128)S(1)} all-to-all(f32[16,4,128]{2,1,0:T(4,128)S(1)} %sums.1), channel_id=1, replica_groups=mesh['fs'=16,'rep'=4,'tp_0'=4,'tp_1'=2] {'rep','tp_0'}, dimensions={0} | all-to-all | bytes 65536 | tf_op jit(solution)/shard_map/sums/all_to_all | solution.py:34
  118.4 0.0 copy-done.2
  118.4 0.0 copy-done.4
  118.4 1.1 update.1
  (3 shorter events, 0.1 us)
Async XLA Ops:
  4.8 5.0 %copy-start.5 = (bf16[1,16,256]{2,1,0:T(8,128)(2,1)S(1)}, bf16[1,16,256]{2,1,0:T(8,128)(2,1)}, u32[]{:S(2)}) copy-start(bf16[1,16,256]{2,1,0:T(8,128)(2,1)} %param.20) | copy-start | bytes 24580
  4.8 36.7 %all-to-all-start = ((f32[4,640,256]{2,1,0:T(8,128)}), f32[4,640,256]{2,1,0:T(8,128)S(1)}, u32[]{:S(2)}, u32[]{:S(2)}) async-start(f32[4,640,256]{2,1,0:T(8,128)} %product.1), calls=%async_computation | async-start | bytes 5242880 | tf_op jit(solution)/shard_map/near/all_to_all | solution.py:34
  41.6 41.2 %copy-start = (bf16[256,256]{1,0:T(8,128)(2,1)S(1)}, bf16[256,256]{1,0:T(8,128)(2,1)}, u32[]{:S(2)}) copy-start(bf16[256,256]{1,0:T(8,128)(2,1)} %rec_right.1) | copy-start | bytes 393220
  41.6 41.2 %copy-start.1 = (f32[128,256]{1,0:T(8,128)S(1)}, f32[128,256]{1,0:T(8,128)}, u32[]{:S(2)}) copy-start(f32[128,256]{1,0:T(8,128)} %rec_moment.1) | copy-start | bytes 393220
  41.6 41.2 %copy-start.3 = (f32[1,16,256]{2,1,0:T(8,128)S(1)}, f32[1,16,256]{2,1,0:T(8,128)}, u32[]{:S(2)}) copy-start(f32[1,16,256]{2,1,0:T(8,128)} %param.19) | copy-start | bytes 49156
  42.0 76.4 %copy-start.2 = (f32[128,256]{1,0:T(8,128)S(1)}, f32[128,256]{1,0:T(8,128)}, u32[]{:S(2)}) copy-start(f32[128,256]{1,0:T(8,128)} %rec_weight.1) | copy-start | bytes 393220
  42.0 76.4 %copy-start.4 = (f32[1,16,256]{2,1,0:T(8,128)S(1)}, f32[1,16,256]{2,1,0:T(8,128)}, u32[]{:S(2)}) copy-start(f32[1,16,256]{2,1,0:T(8,128)} %param.18) | copy-start | bytes 49156
  83.9 23.5 %all-to-all-start.3 = ((f32[32,4,128]{2,1,0:T(4,128)}), f32[32,4,128]{2,1,0:T(4,128)S(1)}, u32[]{:S(2)}, u32[]{:S(2)}) async-start(f32[32,4,128]{2,1,0:T(4,128)} %get-tuple-element.18), calls=%async_computation.3 | async-start | bytes 131072 | tf_op jit(solution)/shard_map/sums/all_to_all | solution.py:34
